TPU v7x, 256 devices: a whole 4x4x8 slice. The times are simulated.
256 devices in a mesh: ep: 16 (over y, x), tp: 16 (over z, core).
Axes of the slice: x: 4, y: 4, z: 8, core: 2. Of those that a mesh axis runs over, the one named last changes fastest.
Arguments:
- mixer_in: bfloat16 [65536, 2048], P(('ep', 'tp')), may hold values from -6 to 6
- pre_gain: float32 [2048], replicated, may hold values from 0.1 to 1.9
- glu_value: bfloat16 [2048, 1024], P(None, 'tp'), may hold values from -0.125 to 0.125
- glu_gate: bfloat16 [2048, 1024], P(None, 'tp'), may hold values from -0.125 to 0.125
- conv_kernel: float32 [31, 1024], replicated, may hold values from -1 to 1
- chan_gain: float32 [1024], replicated, may hold values from 0.1 to 1.9
- out_weight: bfloat16 [1024, 2048], P(None, 'tp'), may hold values from -0.1875 to 0.1875
- mix_gain: float32 [2048], replicated, may hold values from 0.1 to 1.9
- expert_in: bfloat16 [8192, 2048], P(('ep', 'tp')), may hold values from -6 to 6
- ffn_gain: float32 [2048], replicated, may hold values from 0.1 to 1.9
- routing: int32 [8192, 2], P(('ep', 'tp')), may hold values from 0 to 31, all different within a row; in each aligned block of 32 rows (0 to 31, 32 to 63, ...) at most 3 rows name the same one
- route_weight: float32 [8192, 2], P(('ep', 'tp')), may hold values from 0.1 to 1
- gate_proj: bfloat16 [32, 2048, 4096], P('ep', None, 'tp'), may hold values from -0.375 to 0.375
- up_proj: bfloat16 [32, 2048, 4096], P('ep', None, 'tp'), may hold values from -0.375 to 0.375
- down_proj: bfloat16 [32, 4096, 2048], P('ep', 'tp'), may hold values from -0.09375 to 0.09375
- expert_gain: float32 [2048], replicated, may hold values from 0.1 to 1.9
Outputs:
- mixed: bfloat16 [65536, 2048], P(('ep', 'tp'))
- routed: bfloat16 [8192, 2048], P(('ep', 'tp'))
Inputs may be any that keep to these rules, and one draw needn't show every extreme that they name: `routing`: each row names 2 different experts; in each aligned block of 32 rows (the rows of one device) no expert is named more than 3 times.
All inputs are finite; a program needn't handle non-finite values.
Results may differ from a plain program's by a relative error of at most 0.02.
Values may be sent and summed in bfloat16 or wider, within the bound.
A program may use at most 128 MiB of HBM per device.

v0:
```python
import jax
import jax.numpy as jnp
from jax import lax
from jax.sharding import PartitionSpec as P

RMS_EPSILON = 1e-06
LAYER_EPSILON = 1e-05
CLAMP_LIMIT = 7.0
SWISH_ALPHA = 1.702


def in_one_piece(arrays, axis, dim, along):
    both = jnp.concatenate(arrays, axis=along)
    out, at, outs = (lax.all_gather(both, axis, axis=dim, tiled=True), 0, [])
    for a in arrays:
        outs.append(lax.slice_in_dim(out, at, at + a.shape[along], axis=along))
        at += a.shape[along]
    return tuple(outs)


def passed_along(value, axis, steps):
    count = lax.axis_size(axis)
    initial, last = (max(0, -steps), min(count, count - steps))
    return lax.ppermute(value, axis, [(source, source + steps) for source in range(initial, last)])


def rms_scale(values, gain_row):
    values = values.astype(jnp.float32)
    return (
        values
        * lax.rsqrt(jnp.mean(values * values, axis=-1, keepdims=True) + RMS_EPSILON)
        * gain_row
    )


def on_device(
    mixer_in,
    pre_gain,
    glu_value,
    glu_gate,
    conv_kernel,
    chan_gain,
    out_weight,
    mix_gain,
    expert_in,
    ffn_gain,
    routing,
    route_weight,
    gate_proj,
    up_proj,
    down_proj,
    expert_gain,
):
    groups_ep = lax.axis_size("ep")
    local_experts = gate_proj.shape[0]
    experts = local_experts * groups_ep
    token_rows, top_count = routing.shape
    capacity = max(2, 3 * token_rows * top_count // (2 * experts))
    flat_route = routing.reshape(-1)
    onehot = (flat_route[:, None] == jnp.arange(experts, dtype=jnp.int32)[None, :]).astype(
        jnp.int32
    )
    before = jnp.cumsum(onehot, axis=0) - onehot
    rank_within = jnp.sum(before * onehot, axis=1)
    slot_index = (flat_route * capacity + rank_within).reshape(token_rows, top_count)
    slot_ids = jnp.arange(experts * capacity, dtype=jnp.int32)
    chosen = slot_index[None, :, :] == slot_ids[:, None, None]
    pick_matrix = jnp.sum(chosen.astype(jnp.float32), axis=2).astype(jnp.bfloat16)
    normed_exp = rms_scale(expert_in, ffn_gain).astype(jnp.bfloat16)
    outgoing = jnp.dot(pick_matrix, normed_exp, preferred_element_type=jnp.float32).astype(
        jnp.bfloat16
    )
    outgoing = outgoing.reshape(groups_ep, local_experts * capacity, outgoing.shape[1])
    arrived = lax.all_to_all(outgoing, "ep", split_axis=0, concat_axis=0, tiled=True)
    value_full, gate_full, out_full, every_row = (
        *in_one_piece((glu_value, glu_gate), "tp", 1, 0),
        lax.all_gather(out_weight, "tp", axis=1, tiled=True),
        lax.all_gather(arrived, "tp", axis=0, tiled=True),
    )
    row_block = every_row.reshape(every_row.shape[0], local_experts, capacity, every_row.shape[2])
    gate_pre = jnp.einsum(
        "xecd,edf->xecf", row_block, gate_proj, preferred_element_type=jnp.float32
    )
    up_pre = jnp.einsum("xecd,edf->xecf", row_block, up_proj, preferred_element_type=jnp.float32)
    gate_pre = jnp.minimum(gate_pre, CLAMP_LIMIT)
    up_pre = jnp.clip(up_pre, -CLAMP_LIMIT, CLAMP_LIMIT)
    hidden_act = ((up_pre + 1.0) * gate_pre * jax.nn.sigmoid(SWISH_ALPHA * gate_pre)).astype(
        jnp.bfloat16
    )
    normed_mix = rms_scale(mixer_in, pre_gain).astype(jnp.bfloat16)
    value_pre = jnp.dot(normed_mix, value_full, preferred_element_type=jnp.float32)
    gate_mix = jnp.dot(normed_mix, gate_full, preferred_element_type=jnp.float32)
    gated_rows = (value_pre * jax.nn.sigmoid(gate_mix)).astype(jnp.bfloat16)
    kernel_width = conv_kernel.shape[0]
    length = gated_rows.shape[0]
    rim_rows = passed_along(gated_rows[length - (kernel_width - 1) :], ("ep", "tp"), 1)
    padded = jnp.concatenate([rim_rows, gated_rows], axis=0).astype(jnp.float32)
    conv_sum = jnp.zeros((length, gated_rows.shape[1]), jnp.float32)
    for offset in range(kernel_width):
        conv_sum = conv_sum + conv_kernel[offset] * padded[offset : offset + length]
    row_mean = jnp.mean(conv_sum, axis=-1, keepdims=True)
    centred = conv_sum - row_mean
    row_var = jnp.mean(centred * centred, axis=-1, keepdims=True)
    activated = jax.nn.silu(centred * lax.rsqrt(row_var + LAYER_EPSILON) * chan_gain).astype(
        jnp.bfloat16
    )
    projected = jnp.dot(activated, out_full, preferred_element_type=jnp.float32)
    mixed = rms_scale(projected, mix_gain).astype(jnp.bfloat16)
    summed = lax.psum_scatter(
        jnp.einsum(
            "xecf,efd->xecd", hidden_act, down_proj, preferred_element_type=jnp.float32
        ).astype(jnp.bfloat16),
        "tp",
        scatter_dimension=0,
        tiled=True,
    )
    returned = lax.all_to_all(summed, "ep", split_axis=0, concat_axis=0, tiled=True)
    returned = returned.reshape(experts * capacity, returned.shape[3])
    combined = jnp.zeros((token_rows, returned.shape[1]), jnp.float32)
    for column in range(top_count):
        combined = combined + route_weight[:, column][:, None] * returned[
            slot_index[:, column]
        ].astype(jnp.float32)
    routed = rms_scale(combined, expert_gain).astype(jnp.bfloat16)
    return (mixed, routed)


def solution(mesh):
    in_specs = (
        P(("ep", "tp"), None),
        P(),
        P(None, "tp"),
        P(None, "tp"),
        P(),
        P(),
        P(None, "tp"),
        P(),
        P(("ep", "tp"), None),
        P(),
        P(("ep", "tp"), None),
        P(("ep", "tp"), None),
        P("ep", None, "tp"),
        P("ep", None, "tp"),
        P("ep", "tp", None),
        P(),
    )
    out_specs = (P(("ep", "tp"), None), P(("ep", "tp"), None))
    return jax.shard_map(
        on_device, mesh=mesh, in_specs=in_specs, out_specs=out_specs, check_vma=False
    )
```

profile of v0, /device:TPU:1, one launch (start us, length us, event | category | flops | bytes accessed | tf_op | source)
XLA Modules:
  0.0 275.1 jit_solution(17513660276192027920)
XLA Ops:
  7.2 0.0 all-gather.8.cloned.1.call-start
  7.2 0.9 copy.45
  8.2 0.1 eq.28
  8.3 0.1 fusion.84
  8.3 0.1 reduce_window_sum.11
  8.4 0.2 select_reduce_fusion
  8.6 0.1 reduce_sum.79
  8.7 0.1 copy.46
  8.8 0.7 multiply_add_fusion.1
  9.5 0.1 convert_reduce_fusion
  9.6 1.0 fusion.78
  10.6 1.2 convolution_convert_fusion
  11.9 0.1 reshape.72
  12.0 17.8 %all_to_all.10 = bf16[16,6,2048]{2,1,0:T(8,128)(2,1)S(1)} all-to-all(bf16[16,6,2048]{2,1,0:T(8,128)(2,1)S(1)} %reshape.72), channel_id=1, replica_groups=mesh['ep'=16,'tp'=16] {'ep'}, dimensions={0} | all-to-all | bytes 786432 | tf_op jit(solution)/shard_map/all_to_all | solution.py:74
  29.8 1.0 copy.47
  30.9 0.0 all-gather.4.cloned.1.call-start
  30.9 0.8 pad_maximum_fusion
  31.8 0.0 all-gather.6.cloned.1.call-start
  31.8 0.7 all-gather.6.cloned.1.call-update
  32.5 0.0 reduce-scatter.2.cloned.1.call-start
  32.6 45.4 %all-gather.8.cloned.1.call-done = bf16[256,6,2048]{2,0,1:T(8,128)(2,1)} async-done(((bf16[16,6,2048]{2,0,1:T(8,128)(2,1)}), bf16[256,6,2048]{2,0,1:T(8,128)(2,1)}) %all-gather.8.cloned.1.call-update) | async-done | bytes 6291472 | tf_op jit(solution)/shard_map/all_gather | solution.py:78
  77.9 6.4 %fusion.8 = f32[2,256,3,256]{3,1,2,0:T(8,128)} fusion(bf16[256,2,3,2048]{3,0,2,1:T(8,128)(2,1)} %bitcast.102, bf16[2,2048,256]{2,1,0:T(8,128)(2,1)} %param.28), kind=kOutput, calls=%fused_computation.14 | convolution fusion | flops 1610612736 | bytes 9961472 | tf_op jit(solution)/shard_map/xecd,edf->xecf/dot_general | solution.py:81
  84.4 10.3 %convert_bitcast_fusion = bf16[256,2,3,2048]{3,0,2,1:T(8,128)(2,1)} fusion(bf16[2,256,2048]{2,1,0:T(8,128)(2,1)S(1)} %copy-done, f32[2,256,3,256]{3,1,2,0:T(8,128)} %fusion.8, bf16[256,2,3,2048]{3,0,2,1:T(8,128)(2,1)} %bitcast.103, bf16[2,2048,256]{2,1,0:T(8,128)(2,1)} %param.29), kind=kOutput, calls=%fused_computation.2 | convolution fusion | flops 3228303360 | bytes 18350080 | tf_op jit(solution)/shard_map/xecf,efd->xecd/dot_general | solution.py:110
  94.7 1.2 copy-done.1
  95.9 0.3 fusion.4
  96.3 0.1 fusion.95
  96.3 38.5 %all-gather.4.cloned.1.call-done = bf16[4096,1024]{0,1:T(8,128)(2,1)} async-done(((bf16[4096,64]{0,1:T(8,128)(2,1)}), bf16[4096,1024]{0,1:T(8,128)(2,1)}) %all-gather.4.cloned.1.call-update) | async-done | bytes 8388624 | tf_op jit(solution)/shard_map/all_gather | solution.py:14
  134.8 3.8 %fusion.34 = f32[256,1024]{1,0:T(8,128)S(1)} fusion(bf16[4096,1024]{0,1:T(8,128)(2,1)} %all-gather.4.cloned.1.call-done, bf16[256,2048]{1,0:T(8,128)(2,1)S(1)} %copy-done.1, f32[2048]{0:T(1024)S(1)} %copy-done.9, f32[256]{0:T(256)S(1)} %add_rsqrt_fusion.2), kind=kOutput, calls=%fused_computation.27 | convolution fusion | flops 1076625408 | bytes 6300672 | tf_op jit(solution)/shard_map/dot_general | solution.py:92
  138.7 0.8 copy-done.8
  139.5 1.3 fusion.26
  140.8 2.1 collective-permute-start
  142.9 1.1 collective-permute-done
  144.1 0.2 maximum_convert_fusion
  144.2 5.4 %fusion.93 = (f32[256]{0:T(256)S(1)}, f32[256,1024]{1,0:T(8,128)S(1)}) fusion(f32[286,1024]{1,0:T(8,128)S(1)} %maximum_convert_fusion, f32[1024]{0:T(1024)S(1)} %bitcast.81, f32[1024]{0:T(1024)S(1)} %bitcast.82, f32[1024]{0:T(1024)S(1)} %bitcast.84, f32[1024]{0:T(1024)S(1)} %bitcast.85, f32[1024]{0:T(1024)S(1)} %bitcast.86, f32[1024]{0:T(1024)S(1)} %bitcast.87, ...), kind=kLoop, calls=%fused_computation.138 | loop fusion | flops 16252672 | bytes 33682432 | tf_op jit(solution)/shard_map/reduce_sum | solution.py:101
  149.7 0.2 multiply_reduce_fusion.1
  150.0 34.5 %all-gather.6.cloned.1.call-done = bf16[1024,2048]{1,0:T(8,128)(2,1)} async-done(((bf16[1024,128]{1,0:T(8,128)(2,1)}), bf16[1024,2048]{1,0:T(8,128)(2,1)}) %all-gather.6.cloned.1.call-update) | async-done | bytes 4194320 | tf_op jit(solution)/shard_map/all_gather | solution.py:77
  184.5 5.0 %multiply_reduce_fusion = (f32[256]{0:T(256)S(1)}, f32[256,2048]{1,0:T(8,128)}) fusion(bf16[1024,2048]{1,0:T(8,128)(2,1)} %all-gather.6.cloned.1.call-done, f32[256,1024]{1,0:T(8,128)S(1)} %get-tuple-element.3, f32[1024]{0:T(1024)S(1)} %copy-done.10, f32[256]{0:T(256)S(1)} %add_rsqrt_fusion.1, f32[256]{0:T(256)S(1)} %broadcast_multiply_fusion), kind=kOutput, calls=%fused_computation.19 | convolution fusion | flops 1076887296 | bytes 7347200 | tf_op jit(solution)/shard_map/dot_general | solution.py:107
  189.5 59.1 %reduce-scatter.2.cloned.1.call-done = bf16[16,2,3,2048]{3,0,2,1:T(8,128)(2,1)} async-done(((bf16[256,2,3,2048]{3,0,2,1:T(8,128)(2,1)}), bf16[16,2,3,2048]{3,0,2,1:T(8,128)(2,1)}) %reduce-scatter.2.cloned.1.call-update) | async-done | bytes 393232 | tf_op jit(solution)/shard_map/reduce_scatter | solution.py:109
  248.7 2.2 copy.48
  250.8 6.5 %all-to-all-start.1 = ((bf16[16,2,3,2048]{3,1,2,0:T(2,128)(2,1)}), bf16[16,2,3,2048]{3,1,2,0:T(2,128)(2,1)S(1)}, u32[]{:S(2)}, u32[]{:S(2)}) async-start(bf16[16,2,3,2048]{3,1,2,0:T(2,128)(2,1)} %copy.48), calls=%async_computation.2 | async-start | bytes 786432 | tf_op jit(solution)/shard_map/all_to_all | solution.py:117
  257.3 2.8 %multiply_convert_fusion = bf16[256,2048]{1,0:T(8,128)(2,1)} fusion(f32[256,2048]{1,0:T(8,128)} %get-tuple-element.40, f32[2048]{0:T(1024)S(1)} %copy-done.5, f32[256]{0:T(256)S(1)} %add_rsqrt_fusion), kind=kLoop, calls=%fused_computation.18 | loop fusion | flops 1572864 | bytes 3154944 | tf_op jit(solution)/shard_map/convert_element_type | solution.py:108
  260.1 5.4 %all-to-all-done.1 = bf16[16,2,3,2048]{3,1,2,0:T(2,128)(2,1)S(1)} async-done(((bf16[16,2,3,2048]{3,1,2,0:T(2,128)(2,1)}), bf16[16,2,3,2048]{3,1,2,0:T(2,128)(2,1)S(1)}, u32[]{:S(2)}, u32[]{:S(2)}) %all-to-all-start.1) | async-done | bytes 393248 | tf_op jit(solution)/shard_map/all_to_all | solution.py:117
  265.6 0.3 copy.49
  265.9 0.3 reshape.74
  266.2 0.7 gather_fusion
  266.9 0.7 gather_fusion.1
  267.5 0.2 multiply_reduce_fusion.2
  267.8 0.8 multiply_convert_fusion.4
  (34 shorter events, 0.2 us)
Async XLA Ops:
  7.2 77.2 %copy-start = (bf16[2,256,2048]{2,1,0:T(8,128)(2,1)S(1)}, bf16[2,256,2048]{2,1,0:T(8,128)(2,1)}, u32[]{:S(2)}) copy-start(bf16[2,256,2048]{2,1,0:T(8,128)(2,1)} %param.30) | copy-start | bytes 6291460
  7.2 23.7 %copy-start.3 = (bf16[2048,64]{0,1:T(8,128)(2,1)S(1)}, bf16[2048,64]{0,1:T(8,128)(2,1)}, u32[]{:S(2)}) copy-start(bf16[2048,64]{0,1:T(8,128)(2,1)} %param.18) | copy-start | bytes 786436
  7.2 23.7 %copy-start.2 = (bf16[2048,64]{0,1:T(8,128)(2,1)S(1)}, bf16[2048,64]{0,1:T(8,128)(2,1)}, u32[]{:S(2)}) copy-start(bf16[2048,64]{0,1:T(8,128)(2,1)} %param.19) | copy-start | bytes 786436
  7.2 70.7 %all-gather.8.cloned.1.call-start = ((), (), s32[]{:S(2)}) async-start(), calls=%async_computation.5 | async-start | bytes 6684672 | tf_op jit(solution)/shard_map/all_gather | solution.py:78
  30.9 104.0 %all-gather.4.cloned.1.call-start = ((), (), s32[]{:S(2)}) async-start(), calls=%async_computation.3 | async-start | bytes 8912896 | tf_op jit(solution)/shard_map/all_gather | solution.py:14
  31.8 152.7 %all-gather.6.cloned.1.call-start = ((), (), s32[]{:S(2)}) async-start(), calls=%async_computation.4 | async-start | bytes 4456448 | tf_op jit(solution)/shard_map/all_gather | solution.py:77
  32.5 216.2 %reduce-scatter.2.cloned.1.call-start = ((), (), s32[]{:S(2)}) async-start(), calls=%async_computation.6 | async-start | bytes 6684672 | tf_op jit(solution)/shard_map/reduce_scatter | solution.py:109
  94.6 1.2 copy-start.1
  94.7 1.5 copy-start.7
  94.7 1.6 copy-start.4
  94.7 40.2 %copy-start.9 = (f32[2048]{0:T(1024)S(1)}, f32[2048]{0:T(1024)}, u32[]{:S(2)}) copy-start(f32[2048]{0:T(1024)} %param.17) | copy-start | bytes 24580
  134.8 4.6 %copy-start.8 = (bf16[4096,1024]{0,1:T(8,128)(2,1)S(1)}, bf16[4096,1024]{0,1:T(8,128)(2,1)}, u32[]{:S(2)}) copy-start(bf16[4096,1024]{0,1:T(8,128)(2,1)} %all-gather.4.cloned.1.call-done) | copy-start | bytes 25165828
  140.8 3.2 %collective-permute-start = (bf16[30,1024]{1,0:T(8,128)(2,1)S(1)}, bf16[30,1024]{1,0:T(8,128)(2,1)S(1)}, u32[]{:S(2)}, u32[]{:S(2)}) collective-permute-start(bf16[30,1024]{1,0:T(8,128)(2,1)S(1)} %slice.282), channel_id=1, source_target_pairs={{0,1},{1,2},{2,3},{3,4},{4,5},{5,6},{6,7},{7,8},{8,9},{9,10},{10,1... | collective-permute-start | bytes 184328 | tf_op jit(solution)/shard_map/ppermute | solution.py:24
  144.2 40.3 %copy-start.10 = (f32[1024]{0:T(1024)S(1)}, f32[1024]{0:T(1024)}, u32[]{:S(2)}) copy-start(f32[1024]{0:T(1024)} %param.21) | copy-start | bytes 12292
  150.0 107.4 %copy-start.5 = (f32[2048]{0:T(1024)S(1)}, f32[2048]{0:T(1024)}, u32[]{:S(2)}) copy-start(f32[2048]{0:T(1024)} %param.23) | copy-start | bytes 24580
  250.8 14.8 %all-to-all-start.1 = ((bf16[16,2,3,2048]{3,1,2,0:T(2,128)(2,1)}), bf16[16,2,3,2048]{3,1,2,0:T(2,128)(2,1)S(1)}, u32[]{:S(2)}, u32[]{:S(2)}) async-start(bf16[16,2,3,2048]{3,1,2,0:T(2,128)(2,1)} %copy.48), calls=%async_computation.2 | async-start | bytes 786432 | tf_op jit(solution)/shard_map/all_to_all | solution.py:117
  260.1 7.6 %copy-start.6 = (f32[2048]{0:T(1024)S(1)}, f32[2048]{0:T(1024)}, u32[]{:S(2)}) copy-start(f32[2048]{0:T(1024)} %param.31) | copy-start | bytes 24580
Sparse Core Ops, SparseCore 0:
  31.0 46.9 all-gather.7
  80.3 54.4 all-gather.3
  136.6 47.8 all-gather.5
  186.9 61.7 reduce-scatter.1
where the time goes:
time: 278 us; the launch traced here: 275 us
  waiting for transfers between devices  185 us (67%)
  matrix products  28.1 us (10%)
  blocking collectives  17.8 us (6%)
  between operations  14 us (5%)
  other arithmetic  13 us (5%)
  starting transfers between devices  8.76 us (3%)
  local copies, waits for them, and re-layouts  8.58 us (3%)
    reduce_scatter x1, waiting for transfers between devices, on_device(): lax.psum_scatter(jnp.einsum('xecf,efd->xecd', hidden_act, down_proj, pref...  59.1 us
    all_gather x1, waiting for transfers between devices, on_device(): lax.all_gather(arrived, 'tp', axis=0, tiled=True)  45.4 us
    all_gather x1, waiting for transfers between devices, in_one_piece(): out, at, outs = (lax.all_gather(both, axis, axis=dim, tiled=True), 0, [])  38.5 us
    all_gather x1, waiting for transfers between devices, on_device(): lax.all_gather(out_weight, 'tp', axis=1, tiled=True)  34.5 us
    all_to_all x1, blocking collectives, on_device(): lax.all_to_all(outgoing, 'ep', split_axis=0, concat_axis=0, tiled=True)  17.8 us
    dot_general x1, matrix products, on_device(): jnp.einsum('xecf,efd->xecd', hidden_act, down_proj, preferred_element_typ...  10.3 us
    all_to_all x1, starting transfers between devices, on_device(): lax.all_to_all(summed, 'ep', split_axis=0, concat_axis=0, tiled=True)  6.5 us
    dot_general x1, matrix products, on_device(): jnp.einsum('xecd,edf->xecf', row_block, gate_proj, preferred_element_type...  6.43 us
  transfers between devices with their start and end apart: 6, of which 6 were waited for; matrix products, arithmetic and copies ran while one was open for 13% of the time, Pallas kernels for 0%

commit v1 on v0

v1 whole, which is shorter than its diff:
```python
import functools

import jax
import jax.numpy as jnp
from jax import lax
from jax.experimental import pallas as pl
from jax.experimental.pallas import tpu as pltpu
from jax.sharding import PartitionSpec as P

RMS_EPSILON = 1e-06
LAYER_EPSILON = 1e-05
CLAMP_LIMIT = 7.0
SWISH_ALPHA = 1.702
CAPS = 3
MESH = pl.DeviceIdType.MESH
F32 = jnp.float32
BF16 = jnp.bfloat16


def iota(shape, dim):
    return lax.broadcasted_iota(jnp.int32, shape, dim)


def mm(a, b):
    return jnp.dot(a, b, preferred_element_type=F32)


def rms_scale(values, gain_row):
    values = values.astype(F32)
    return (
        values
        * lax.rsqrt(jnp.mean(values * values, axis=-1, keepdims=True) + RMS_EPSILON)
        * gain_row
    )


def expert_kernel(
    n_ep,
    n_z,
    x_ref,
    fgain_ref,
    route_ref,
    rw_ref,
    egain_ref,
    gate_hbm,
    up_hbm,
    down_hbm,
    out_ref,
    gate_v,
    up_v,
    down_v,
    slab,
    arrived,
    rows,
    parts,
    mate,
    ring_in,
    back_slab,
    back,
    w_sem,
    a_send,
    a_recv,
    g_send,
    g_recv,
    m_send,
    m_recv,
    q_send,
    q_recv,
    s_send,
    s_recv,
    b_send,
    b_recv,
):
    half_z = n_z // 2
    tokens, width = x_ref.shape
    half = width // 2
    cap = n_ep * CAPS
    slots = n_ep * 16
    ep, tp = lax.axis_index("ep"), lax.axis_index("tp")
    z, core = tp // 2, tp % 2
    mate_tp = 2 * z + 1 - core
    next_tp = 2 * ((z + 1) % n_z) + core
    prev_tp = 2 * ((z + n_z - 1) % n_z) + core
    toward = {1: next_tp, -1: prev_tp}
    side = {1: 0, -1: 1}

    def pos(d):
        d = (d + half_z - 1) % n_z - (half_z - 1)
        return 2 * d - 1 if d > 0 else -2 * d

    def place(d):
        return n_z - 1 if d in (half_z, -half_z) else pos(d)

    def hops(way, e):
        return half_z if (way == 1) == (e == 0) else half_z - 1

    loads = [
        pltpu.make_async_copy(src, dst, w_sem.at[i])
        for i, (src, dst) in enumerate(
            ((gate_hbm, gate_v), (up_hbm, up_v), (down_hbm, down_v))
        )
    ]
    for load in loads:
        load.start()

    barrier = pltpu.get_barrier_semaphore()

    def greet(i, carry):
        pl.semaphore_signal(
            barrier, inc=1, device_id=((ep + i) % n_ep, tp), device_id_type=MESH
        )
        return carry

    lax.fori_loop(1, n_ep, greet, 0)
    for other in (mate_tp, next_tp, prev_tp):
        pl.semaphore_signal(
            barrier, inc=1, device_id=(ep, other), device_id_type=MESH
        )

    experts = 2 * n_ep
    chosen = [route_ref[:, k : k + 1] for k in range(2)]
    named = [
        (c == iota((tokens, experts), 1)).astype(F32) for c in chosen
    ]
    earlier = (iota((tokens, tokens), 1) < iota((tokens, tokens), 0)).astype(F32)
    before = mm(earlier.astype(BF16), (named[0] + named[1]).astype(BF16))
    spot = [
        (c // 2) * 16
        + (c % 2) * CAPS
        + jnp.sum(before * n, axis=1, keepdims=True).astype(jnp.int32)
        for c, n in zip(chosen, named)
    ]
    eye = iota((tokens, tokens), 0) == iota((tokens, tokens), 1)
    spot_row = [
        jnp.sum(jnp.where(eye, s.astype(F32), 0.0), axis=0, keepdims=True).astype(
            jnp.int32
        )
        for s in spot
    ]
    normed = rms_scale(x_ref[...], fgain_ref[...]).astype(BF16)
    picked = jnp.zeros((slots, half), F32)
    for h in range(2):
        at = iota((slots, tokens), 0) - 8 * h
        hit = jnp.logical_or(at == spot_row[0], at == spot_row[1])
        picked = picked + mm(
            jnp.where(hit, 1.0, 0.0).astype(BF16), normed[:, h * half : (h + 1) * half]
        )
    slab[...] = picked.astype(BF16).reshape(n_ep, 16, half)
    pl.semaphore_wait(barrier, n_ep - 1 + 3)

    def exchange(src, dst, send, recv):
        def copy(i):
            peer = (ep + i) % n_ep
            return pltpu.make_async_remote_copy(
                src_ref=src.at[peer],
                dst_ref=dst.at[ep],
                send_sem=send.at[i],
                recv_sem=recv.at[i],
                device_id=(peer, tp),
                device_id_type=MESH,
            )

        return copy

    def run(fn, low, high):
        def body(i, carry):
            fn(i)
            return carry

        lax.fori_loop(low, high, body, 0)

    out_copy = exchange(slab, arrived, a_send, a_recv)
    run(lambda i: out_copy(i).start(), 1, n_ep)
    arrived[ep] = slab[ep]
    run(lambda i: out_copy(i).wait_recv(), 1, n_ep)

    def to_rows(e, h, shape, row_dim, slot_dim):
        row, slot = iota(shape, row_dim), iota(shape, slot_dim)
        inner = slot % 8 - CAPS * e
        hit = (row == (slot // 16) * CAPS + inner) & ((slot // 8) % 2 == h)
        hit = hit & (inner >= 0) & (inner < CAPS)
        return jnp.where(hit, 1.0, 0.0).astype(BF16)

    def ring(way, e, k):
        return pltpu.make_async_remote_copy(
            src_ref=rows.at[e, place(-way * (k - 1)), 0],
            dst_ref=rows.at[e, place(-way * k), 0],
            send_sem=g_send.at[side[way], e, k - 1],
            recv_sem=g_recv.at[side[way], e, k - 1],
            device_id=(ep, toward[way]),
            device_id_type=MESH,
        )

    def to_mate(e, p):
        return pltpu.make_async_remote_copy(
            src_ref=rows.at[e, p, 0],
            dst_ref=rows.at[e, p, 1],
            send_sem=m_send.at[e, p],
            recv_sem=m_recv.at[e, p],
            device_id=(ep, mate_tp),
            device_id_type=MESH,
        )

    def part_to_mate(e, p):
        return pltpu.make_async_remote_copy(
            src_ref=parts.at[e, p, 1],
            dst_ref=mate.at[e, p],
            send_sem=q_send.at[e, p],
            recv_sem=q_recv.at[e, p],
            device_id=(ep, mate_tp),
            device_id_type=MESH,
        )

    def ring_sum(way, e, k):
        return pltpu.make_async_remote_copy(
            src_ref=parts.at[e, place(way * k), 0],
            dst_ref=ring_in.at[side[way], e, k - 1],
            send_sem=s_send.at[side[way], e, k - 1],
            recv_sem=s_recv.at[side[way], e, k - 1],
            device_id=(ep, toward[way]),
            device_id_type=MESH,
        )

    block = arrived[...].reshape(slots, half)
    for e in range(2):
        for h in range(2):
            rows[e, 0, 0, :, h * half : (h + 1) * half] = mm(
                to_rows(e, h, (cap, slots), 0, 1), block
            ).astype(BF16)
        for way in (1, -1):
            ring(way, e, 1).start()
        to_mate(e, 0).start()
    for load in loads:
        load.wait()

    def ffn(low, high):
        for e in range(2):
            for p in range(low, high):
                to_mate(e, p).wait_recv()
        count = (high - low) * 2 * cap

        def one(e, carry):
            block = rows[e, low:high].reshape(count, width)
            gate = jnp.minimum(mm(block, gate_v[e]), CLAMP_LIMIT)
            up = jnp.clip(mm(block, up_v[e]), -CLAMP_LIMIT, CLAMP_LIMIT)
            hidden = ((up + 1.0) * gate * jax.nn.sigmoid(SWISH_ALPHA * gate)).astype(
                BF16
            )
            parts[e, low:high] = (
                mm(hidden, down_v[e])
                .astype(BF16)
                .reshape(high - low, 2, cap, width)
            )
            return carry

        lax.fori_loop(0, 2, one, 0)
        for e in range(2):
            for p in range(low, high):
                part_to_mate(e, p).start()

    def chip_sum(low, high):
        for e in range(2):
            for p in range(low, high):
                part_to_mate(e, p).wait_recv()
                parts[e, p, 0] = (
                    parts[e, p, 0].astype(F32) + mate[e, p].astype(F32)
                ).astype(BF16)

    ffn(0, 1)
    for k in range(1, half_z + 1):
        for e in range(2):
            for way in (1, -1):
                if k <= hops(way, e):
                    ring(way, e, k).wait_recv()
                    if k < hops(way, e):
                        ring(way, e, k + 1).start()
                    to_mate(e, place(-way * k)).start()
        if k < half_z:
            ffn(2 * k - 1, 2 * k + 1)
            if k == half_z - 1:
                chip_sum(0, 2 * k + 1)
                for e in range(2):
                    for way in (1, -1):
                        if hops(way, e) == k:
                            ring_sum(way, e, k).start()
        else:
            ffn(n_z - 1, n_z)
            chip_sum(n_z - 1, n_z)

    for k in range(half_z, 0, -1):
        for e in range(2):
            for way in (1, -1):
                if k < hops(way, e):
                    ring_sum(way, e, k + 1).wait_recv()
                    p = place(way * k)
                    parts[e, p, 0] = (
                        parts[e, p, 0].astype(F32)
                        + ring_in[side[way], e, k].astype(F32)
                    ).astype(BF16)
                    ring_sum(way, e, k).start()
                elif k == half_z and hops(way, e) == k:
                    ring_sum(way, e, k).start()
    done = []
    for e in range(2):
        for way in (1, -1):
            ring_sum(way, e, 1).wait_recv()
        done.append(
            (
                parts[e, 0, 0].astype(F32)
                + ring_in[0, e, 0].astype(F32)
                + ring_in[1, e, 0].astype(F32)
            ).astype(BF16)
        )

    back_rows = jnp.zeros((slots, half), F32)
    for e in range(2):
        for h in range(2):
            back_rows = back_rows + mm(
                to_rows(e, h, (slots, cap), 1, 0), done[e][:, h * half : (h + 1) * half]
            )
    back_slab[...] = back_rows.astype(BF16).reshape(n_ep, 16, half)
    back_copy = exchange(back_slab, back, b_send, b_recv)
    run(lambda i: back_copy(i).start(), 1, n_ep)
    back[ep] = back_slab[ep]
    mixes = []
    for h in range(2):
        at = iota((tokens, slots), 1) - 8 * h
        share = jnp.zeros((tokens, slots), F32)
        for k in range(2):
            share = share + jnp.where(at == spot[k], rw_ref[:, k : k + 1], 0.0)
        high = share.astype(BF16)
        mixes.append((high, (share - high.astype(F32)).astype(BF16)))
    run(lambda i: back_copy(i).wait_recv(), 1, n_ep)
    results = back[...].reshape(slots, half)
    combined = [mm(high, results) + mm(low, results) for high, low in mixes]
    square = sum(jnp.sum(c * c, axis=1, keepdims=True) for c in combined)
    scale = lax.rsqrt(square / width + RMS_EPSILON)
    for h in range(2):
        cols = slice(h * half, (h + 1) * half)
        out_ref[:, cols] = (combined[h] * scale * egain_ref[:, cols]).astype(BF16)

    run(lambda i: out_copy(i).wait_send(), 1, n_ep)
    run(lambda i: back_copy(i).wait_send(), 1, n_ep)
    for e in range(2):
        for way in (1, -1):
            for k in range(1, hops(way, e) + 1):
                ring(way, e, k).wait_send()
                ring_sum(way, e, k).wait_send()
        for p in range(n_z):
            to_mate(e, p).wait_send()
            part_to_mate(e, p).wait_send()


def experts_path(
    expert_in, ffn_gain, routing, route_weight, gate_proj, up_proj, down_proj, expert_gain
):
    n_ep, n_z = lax.axis_size("ep"), lax.axis_size("tp") // 2
    half_z = n_z // 2
    tokens, width = expert_in.shape
    half, cap, hid = width // 2, n_ep * CAPS, gate_proj.shape[2]
    dma = pltpu.SemaphoreType.DMA
    vmem = pl.BlockSpec(memory_space=pltpu.VMEM)
    hbm = pl.BlockSpec(memory_space=pl.ANY)
    return pl.pallas_call(
        functools.partial(expert_kernel, n_ep, n_z),
        out_shape=jax.ShapeDtypeStruct((tokens, width), BF16),
        in_specs=[vmem] * 5 + [hbm] * 3,
        out_specs=vmem,
        scratch_shapes=[
            pltpu.VMEM((2, width, hid), BF16),
            pltpu.VMEM((2, width, hid), BF16),
            pltpu.VMEM((2, hid, width), BF16),
            pltpu.VMEM((n_ep, 16, half), BF16),
            pltpu.VMEM((n_ep, 16, half), BF16),
            pltpu.VMEM((2, n_z, 2, cap, width), BF16),
            pltpu.VMEM((2, n_z, 2, cap, width), BF16),
            pltpu.VMEM((2, n_z, cap, width), BF16),
            pltpu.VMEM((2, 2, half_z, cap, width), BF16),
            pltpu.VMEM((n_ep, 16, half), BF16),
            pltpu.VMEM((n_ep, 16, half), BF16),
            dma((3,)),
            dma((n_ep,)),
            dma((n_ep,)),
            dma((2, 2, half_z)),
            dma((2, 2, half_z)),
            dma((2, n_z)),
            dma((2, n_z)),
            dma((2, n_z)),
            dma((2, n_z)),
            dma((2, 2, half_z)),
            dma((2, 2, half_z)),
            dma((n_ep,)),
            dma((n_ep,)),
        ],
        compiler_params=pltpu.CompilerParams(
            collective_id=0, has_side_effects=True, vmem_limit_bytes=60 * 1024 * 1024
        ),
        cost_estimate=pl.CostEstimate(
            flops=80_000_000_000, bytes_accessed=16_000_000, transcendentals=0
        ),
        name="experts",
    )(
        expert_in,
        ffn_gain.reshape(1, -1),
        routing,
        route_weight,
        expert_gain.reshape(1, -1),
        gate_proj,
        up_proj,
        down_proj,
    )


def passed_along(value, axis, steps):
    count = lax.axis_size(axis)
    initial, last = (max(0, -steps), min(count, count - steps))
    return lax.ppermute(value, axis, [(source, source + steps) for source in range(initial, last)])


def on_device(
    mixer_in,
    pre_gain,
    glu_value,
    glu_gate,
    conv_kernel,
    chan_gain,
    out_weight,
    mix_gain,
    expert_in,
    ffn_gain,
    routing,
    route_weight,
    gate_proj,
    up_proj,
    down_proj,
    expert_gain,
):
    n_ep, n_tp, ep = lax.axis_size("ep"), lax.axis_size("tp"), lax.axis_index("ep")
    width, cols = glu_value.shape
    channels = cols * n_tp
    both = jnp.concatenate([glu_value, glu_gate], axis=1)
    rows_v, rows_o = width // n_ep, channels // n_ep
    piece = jnp.concatenate(
        [
            lax.dynamic_slice_in_dim(both, ep * rows_v, rows_v, 0),
            lax.dynamic_slice_in_dim(out_weight, ep * rows_o, rows_o, 0),
        ],
        axis=0,
    )
    full = lax.all_gather(piece, ("ep", "tp"), axis=0, tiled=False)
    full = full.reshape(n_ep, n_tp, rows_v + rows_o, 2 * cols)
    routed = experts_path(
        expert_in, ffn_gain, routing, route_weight, gate_proj, up_proj, down_proj, expert_gain
    )
    glu_full = full[:, :, :rows_v].transpose(0, 2, 1, 3).reshape(width, n_tp * 2 * cols)
    out_full = full[:, :, rows_v:].transpose(0, 2, 1, 3).reshape(channels, width)
    normed_mix = rms_scale(mixer_in, pre_gain).astype(BF16)
    pre = mm(normed_mix, glu_full).reshape(-1, n_tp, 2, cols)
    gated = pre[:, :, 0] * jax.nn.sigmoid(pre[:, :, 1])
    gated_rows = gated.reshape(-1, channels).astype(BF16)
    kernel_width = conv_kernel.shape[0]
    length = gated_rows.shape[0]
    rim_rows = passed_along(gated_rows[length - (kernel_width - 1) :], ("ep", "tp"), 1)
    padded = jnp.concatenate([rim_rows, gated_rows], axis=0).astype(F32)
    conv_sum = jnp.zeros((length, channels), F32)
    for offset in range(kernel_width):
        conv_sum = conv_sum + conv_kernel[offset] * padded[offset : offset + length]
    row_mean = jnp.mean(conv_sum, axis=-1, keepdims=True)
    centred = conv_sum - row_mean
    row_var = jnp.mean(centred * centred, axis=-1, keepdims=True)
    activated = jax.nn.silu(centred * lax.rsqrt(row_var + LAYER_EPSILON) * chan_gain).astype(BF16)
    projected = mm(activated, out_full)
    mixed = rms_scale(projected, mix_gain).astype(BF16)
    return (mixed, routed)


def solution(mesh):
    in_specs = (
        P(("ep", "tp"), None),
        P(),
        P(None, "tp"),
        P(None, "tp"),
        P(),
        P(),
        P(None, "tp"),
        P(),
        P(("ep", "tp"), None),
        P(),
        P(("ep", "tp"), None),
        P(("ep", "tp"), None),
        P("ep", None, "tp"),
        P("ep", None, "tp"),
        P("ep", "tp", None),
        P(),
    )
    out_specs = (P(("ep", "tp"), None), P(("ep", "tp"), None))
    return jax.shard_map(
        on_device, mesh=mesh, in_specs=in_specs, out_specs=out_specs, check_vma=False
    )
```

time: 278 us -> 232 us (0.83)
  waiting for transfers between devices: 185 us -> 28.7 us
  Pallas kernels: 0 us -> 99.5 us
  local copies, waits for them, and re-layouts: 8.58 us -> 59 us
  matrix products: 28.1 us -> 7.37 us
  blocking collectives: 17.8 us -> 0 us
  starting transfers between devices: 8.76 us -> 2 us
  other arithmetic: 13 us -> 17.3 us
    pallas_call x0 -> x1, Pallas kernels: none -> 99.5 us  [experts_path(): pl.pallas_call(functools.partial(expert_kernel, n_ep, n_z), out_shape=jax...]
    all_gather x3 -> x1, waiting for transfers between devices: 118 us -> 28.7 us  [on_device(): full = lax.all_gather(piece, ('ep', 'tp'), axis=0, tiled=False)]
    reduce_scatter x1 -> x0, waiting for transfers between devices: 59.1 us -> none  [on_device(): lax.psum_scatter(jnp.einsum('xecf,efd->xecd', hidden_act, down_proj, pref...]
    transpose x0 -> x4, local copies, waits for them, and re-layouts: none -> 30.8 us  [the longest x2 24.1 us: on_device(): full[:, :, :rows_v].transpose(0, 2, 1, 3).reshape(width, n_tp * 2 * cols)]
    dot_general x6 -> x2, matrix products: 28.1 us -> 7.37 us  [mm(): return jnp.dot(a, b, preferred_element_type=F32)]
    all_to_all x1 -> x0, blocking collectives: 17.8 us -> none  [on_device(): lax.all_to_all(outgoing, 'ep', split_axis=0, concat_axis=0, tiled=True)]
    unnamed x23 -> x26, local copies, waits for them, and re-layouts: 2.95 us -> 15.7 us
    dot_general x0 -> x1, local copies, waits for them, and re-layouts: none -> 12.3 us  [mm(): return jnp.dot(a, b, preferred_element_type=F32)]
  transfers between devices with their start and end apart: 6 -> 2, of which waited for: 6 -> 1; matrix products, arithmetic and copies ran while one was open for 13% -> 4% of each run, Pallas kernels for 0% -> 44%
where the time goes in v1:
time: 232 us; the launch traced here: 228 us
  Pallas kernels  99.5 us (43%)
  local copies, waits for them, and re-layouts  59 us (25%)
  waiting for transfers between devices  28.7 us (12%)
  other arithmetic  17.3 us (7%)
  between operations  14.3 us (6%)
  matrix products  7.37 us (3%)
    pallas_call x1, Pallas kernels, experts_path(): pl.pallas_call(functools.partial(expert_kernel, n_ep, n_z), out_shape=jax...  99.5 us
    all_gather x1, waiting for transfers between devices, on_device(): full = lax.all_gather(piece, ('ep', 'tp'), axis=0, tiled=False)  28.7 us
    transpose x2, local copies, waits for them, and re-layouts, on_device(): full[:, :, :rows_v].transpose(0, 2, 1, 3).reshape(width, n_tp * 2 * cols)  24.1 us
    unnamed x26, local copies, waits for them, and re-layouts  15.7 us
    reduce_sum x1, other arithmetic, on_device(): row_mean = jnp.mean(conv_sum, axis=-1, keepdims=True)  14.2 us
    dot_general x1, local copies, waits for them, and re-layouts, mm(): return jnp.dot(a, b, preferred_element_type=F32)  12.3 us
    dot_general x2, matrix products, mm(): return jnp.dot(a, b, preferred_element_type=F32)  7.37 us
    transpose x2, local copies, waits for them, and re-layouts, on_device(): full[:, :, rows_v:].transpose(0, 2, 1, 3).reshape(channels, width)  6.71 us
  transfers between devices with their start and end apart: 2, of which 1 were waited for; matrix products, arithmetic and copies ran while one was open for 4% of the time, Pallas kernels for 44%

profile of v1, /device:TPU:1, one launch (start us, length us, event | category | flops | bytes accessed | tf_op | source)
XLA Modules:
  0.0 228.2 jit_solution(6726414546295767397)
XLA Ops:
  7.2 0.0 copy-start
  7.2 0.0 copy-start.6
  7.2 0.0 copy-start.7
  7.2 0.0 all-gather.3.cloned.1.call-start
  7.3 1.2 copy.27
  8.5 1.2 copy.28
  9.7 0.0 copy-done
  9.8 0.1 fusion.50
  9.9 0.6 pad_maximum_fusion
  10.5 0.0 all-gather.3.cloned.1.call-update
  10.5 0.0 copy-done.6
  10.5 0.7 copy.32.route_ref
  11.2 0.0 copy-done.7
  11.2 0.7 copy.33.rw_ref
  11.9 0.0 copy-start.2
  11.9 0.0 copy-start.4
  11.9 99.5 %experts.1 = bf16[32,2048]{1,0:T(8,128)(2,1)} custom-call(bf16[32,2048]{1,0:T(8,128)(2,1)} %x_ref.1, f32[1,2048]{1,0:T(1,128)} %bitcast.101, s32[32,2]{1,0:T(8,128)} %copy.32.route_ref, f32[32,2]{1,0:T(8,128)} %copy.33.rw_ref, f32[1,2048]{1,0:T(1,128)} %bitcast.102, bf16[2,2048,256]{2,1,0:T(8,128)(2,1)} %gate_hbm.1, bf16[2,2048,256]{2,1,0:T(8,128)(2,1)} %up_hbm.1, ...), custom_call_target="tpu_custom_call" | custom-call | flops 80000000000 | bytes 16000000 | tf_op jit(solution)/shard_map/experts/pallas_call | solution.py:364
  111.4 0.0 copy-done.2
  111.5 0.3 fusion.3
  111.7 0.0 copy-done.4
  111.8 0.1 fusion.54
  111.9 28.7 %all-gather.3.cloned.1.call-done = bf16[49152,128]{1,0:T(8,128)(2,1)} async-done(((bf16[192,128]{1,0:T(8,128)(2,1)}), bf16[49152,128]{1,0:T(8,128)(2,1)}) %all-gather.3.cloned.1.call-update) | async-done | bytes 12582928 | tf_op jit(solution)/shard_map/all_gather | solution.py:450
  140.6 10.4 %slice_bitcast_fusion = bf16[16,128,16,128]{3,1,2,0:T(8,128)(2,1)} fusion(bf16[16,16,192,128]{3,2,1,0:T(8,128)(2,1)} %bitcast.64), kind=kLoop, calls=%fused_computation.1 | loop fusion | bytes 16777216 | tf_op jit(solution)/shard_map/transpose | solution.py:455
  151.0 13.6 %copy.29 = bf16[16,128,16,128]{3,2,1,0:T(8,128)(2,1)} copy(bf16[16,128,16,128]{3,1,2,0:T(8,128)(2,1)} %slice_bitcast_fusion) | data formatting | bytes 16777216 | tf_op jit(solution)/shard_map/transpose | solution.py:455
  164.7 11.1 %copy.44 = bf16[256,8,16,128]{3,1,2,0:T(8,128)(2,1)} copy(bf16[256,8,16,128]{3,2,1,0:T(8,128)(2,1)} %bitcast.62) | data formatting | bytes 16777216
  175.8 0.0 copy-start.8
  175.8 12.3 %copy.30 = bf16[2048,2048]{1,0:T(8,128)(2,1)} copy(bf16[2048,2048]{0,1:T(8,128)(2,1)} %bitcast.63) | data formatting | bytes 16777216 | tf_op jit(solution)/shard_map/dot_general | solution.py:25
  188.1 0.0 copy-done.8
  188.1 5.8 %fusion.7 = f32[256,16,2,64]{0,3,2,1:T(8,128)S(1)} fusion(bf16[16,2,64,2048]{3,2,1,0:T(8,128)(2,1)} %bitcast.66, bf16[256,2048]{1,0:T(8,128)(2,1)S(1)} %copy-done.2, f32[2048]{0:T(1024)S(1)} %copy-done.8, f32[256]{0:T(256)S(1)} %add_rsqrt_fusion.2), kind=kOutput, calls=%fused_computation.14 | convolution fusion | flops 2149580800 | bytes 11543552 | tf_op jit(solution)/shard_map/dot_general | solution.py:25
  194.0 0.3 fusion.45
  194.3 0.1 slice.272
  194.4 2.0 collective-permute-start
  196.4 3.2 %slice_bitcast_fusion.1 = bf16[16,64,16,128]{3,1,2,0:T(8,128)(2,1)S(1)} fusion(bf16[16,16,192,128]{3,2,1,0:T(8,128)(2,1)} %bitcast.65), kind=kLoop, calls=%fused_computation.5 | loop fusion | bytes 8388608 | tf_op jit(solution)/shard_map/transpose | solution.py:456
  199.6 3.5 %copy.31 = bf16[16,64,16,128]{3,2,1,0:T(8,128)(2,1)S(1)} copy(bf16[16,64,16,128]{3,1,2,0:T(8,128)(2,1)S(1)} %slice_bitcast_fusion.1) | data formatting | bytes 8388608 | tf_op jit(solution)/shard_map/transpose | solution.py:456
  203.1 0.0 collective-permute-done
  203.1 0.4 maximum_convert_fusion
  203.5 0.0 copy-start.9
  203.5 14.2 %fusion.52 = (f32[256]{0:T(256)S(1)}, f32[256,1024]{0,1:T(8,128)S(1)}) fusion(f32[286,1024]{0,1:T(8,128)S(1)} %maximum_convert_fusion, f32[1024]{0:T(1024)S(1)} %bitcast.80, f32[1024]{0:T(1024)S(1)} %bitcast.81, f32[1024]{0:T(1024)S(1)} %bitcast.83, f32[1024]{0:T(1024)S(1)} %bitcast.84, f32[1024]{0:T(1024)S(1)} %bitcast.85, f32[1024]{0:T(1024)S(1)} %bitcast.86, ...), kind=kLoop, calls=%fused_computation.101 | loop fusion | flops 16252672 | bytes 33682432 | tf_op jit(solution)/shard_map/reduce_sum | solution.py:468
  217.7 0.2 multiply_reduce_fusion.1
  217.9 0.0 copy-done.9
  217.9 0.0 copy-start.5
  217.9 0.0 copy-start.1
  217.9 1.5 multiply_reduce_fusion
  219.5 0.0 copy-done.5
  219.5 1.2 multiply_convert_fusion
  220.7 0.0 copy-done.3
  220.7 0.7 copy.46
  221.4 0.0 copy-done.1
  (7 shorter events, 0.1 us)
Async XLA Ops:
  7.2 2.6 %copy-start = (bf16[1024,128]{1,0:T(8,128)(2,1)S(1)}, bf16[1024,128]{1,0:T(8,128)(2,1)}, u32[]{:S(2)}) copy-start(bf16[1024,128]{1,0:T(8,128)(2,1)} %param.22) | copy-start | bytes 786436
  7.2 3.3 %copy-start.6 = (s32[32,2]{0,1:T(2,128)S(1)}, s32[32,2]{0,1:T(2,128)}, u32[]{:S(2)}) copy-start(s32[32,2]{0,1:T(2,128)} %param.26) | copy-start | bytes 772
  7.2 4.0 %copy-start.7 = (f32[32,2]{0,1:T(2,128)S(1)}, f32[32,2]{0,1:T(2,128)}, u32[]{:S(2)}) copy-start(f32[32,2]{0,1:T(2,128)} %param.27) | copy-start | bytes 772
  7.2 133.4 %all-gather.3.cloned.1.call-start = ((), (), s32[]{:S(2)}) async-start(), calls=%async_computation | async-start | bytes 12632064 | tf_op jit(solution)/shard_map/all_gather | solution.py:450
  11.9 99.5 %copy-start.2 = (bf16[256,2048]{1,0:T(8,128)(2,1)S(1)}, bf16[256,2048]{1,0:T(8,128)(2,1)}, u32[]{:S(2)}) copy-start(bf16[256,2048]{1,0:T(8,128)(2,1)} %param.16) | copy-start | bytes 3145732
  11.9 99.8 %copy-start.4 = (f32[31,1024]{1,0:T(8,128)S(1)}, f32[31,1024]{1,0:T(8,128)}, u32[]{:S(2)}) copy-start(f32[31,1024]{1,0:T(8,128)} %param.20) | copy-start | bytes 380932
  175.8 12.3 %copy-start.8 = (f32[2048]{0:T(1024)S(1)}, f32[2048]{0:T(1024)}, u32[]{:S(2)}) copy-start(f32[2048]{0:T(1024)} %param.17) | copy-start | bytes 24580
  194.4 8.7 %collective-permute-start = (bf16[30,1024]{0,1:T(8,128)(2,1)S(1)}, bf16[30,1024]{0,1:T(8,128)(2,1)S(1)}, u32[]{:S(2)}, u32[]{:S(2)}) collective-permute-start(bf16[30,1024]{0,1:T(8,128)(2,1)S(1)} %bitcast.69), channel_id=1, source_target_pairs={{0,1},{1,2},{2,3},{3,4},{4,5},{5,6},{6,7},{7,8},{8,9},{9,10},{10,1... | collective-permute-start | bytes 184328 | tf_op jit(solution)/shard_map/ppermute | solution.py:417
  203.5 14.4 %copy-start.9 = (f32[1024]{0:T(1024)S(1)}, f32[1024]{0:T(1024)}, u32[]{:S(2)}) copy-start(f32[1024]{0:T(1024)} %param.21) | copy-start | bytes 12292
  217.9 1.6 copy-start.5
  217.9 3.4 %copy-start.1 = (bf16[1024,128]{1,0:T(8,128)(2,1)S(1)}, bf16[1024,128]{1,0:T(8,128)(2,1)}, u32[]{:S(2)}) copy-start(bf16[1024,128]{1,0:T(8,128)(2,1)} %param.22) | copy-start | bytes 786436
  219.5 1.2 copy-start.3
Sparse Core Ops, SparseCore 0:
  12.4 128.1 all-gather.2

commit v2 on v1

v2 whole, which is shorter than its diff:
```python
import functools

import jax
import jax.numpy as jnp
from jax import lax
from jax.experimental import pallas as pl
from jax.experimental.pallas import tpu as pltpu
from jax.sharding import PartitionSpec as P

RMS_EPSILON = 1e-06
LAYER_EPSILON = 1e-05
CLAMP_LIMIT = 7.0
SWISH_ALPHA = 1.702
CAPS = 3
MESH = pl.DeviceIdType.MESH
F32 = jnp.float32
BF16 = jnp.bfloat16


def iota(shape, dim):
    return lax.broadcasted_iota(jnp.int32, shape, dim)


def mm(a, b):
    return jnp.dot(a, b, preferred_element_type=F32)


def rms_scale(values, gain_row):
    values = values.astype(F32)
    return (
        values
        * lax.rsqrt(jnp.mean(values * values, axis=-1, keepdims=True) + RMS_EPSILON)
        * gain_row
    )


def both_kernel(
    n_ep,
    n_z,
    x_ref,
    fgain_ref,
    route_ref,
    rw_ref,
    egain_ref,
    pgain_ref,
    taps_ref,
    cgain_ref,
    mgain_ref,
    gate_hbm,
    up_hbm,
    down_hbm,
    mix_hbm,
    value_hbm,
    glu_hbm,
    ow_hbm,
    out_ref,
    mixed_hbm,
    gate_v,
    up_v,
    down_v,
    mix_v,
    loc_vg,
    loc_o,
    slab,
    arrived,
    rows,
    parts,
    mate,
    ring_in,
    back_slab,
    back,
    vg_all,
    o_all,
    normed_v,
    ext,
    tail_rows,
    rim,
    conv_v,
    act_v,
    proj_v,
    mixed_v,
    w_sem,
    a_send,
    a_recv,
    g_send,
    g_recv,
    m_send,
    m_recv,
    q_send,
    q_recv,
    s_send,
    s_recv,
    b_send,
    b_recv,
    c_send,
    c_recv,
    p_send,
    p_recv,
    t_send,
    t_recv,
    h_sem,
    o_sem,
):
    half_z = n_z // 2
    n_s = 4
    tokens, width = x_ref.shape
    half = width // 2
    cap = n_ep * CAPS
    slots = n_ep * 16
    length = mix_v.shape[0]
    unit = width // n_ep
    o_unit = loc_o.shape[1] // n_ep
    ep, tp = lax.axis_index("ep"), lax.axis_index("tp")
    z, core = tp // 2, tp % 2
    mate_tp = 2 * z + 1 - core
    next_tp = 2 * ((z + 1) % n_z) + core
    prev_tp = 2 * ((z + n_z - 1) % n_z) + core
    toward = {1: next_tp, -1: prev_tp}
    side = {1: 0, -1: 1}
    major = (ep // n_s, ep % n_s)
    minor = (ep % n_s, ep // n_s)
    after = (tp + 1) // (2 * n_z)
    line_next = ((ep + after) % n_ep, (tp + 1) % (2 * n_z))
    behind = (2 * n_z - tp) // (2 * n_z)
    line_prev = ((ep + n_ep - behind) % n_ep, (tp + 2 * n_z - 1) % (2 * n_z))

    def pos(d):
        return 2 * d - 1 if d > 0 else -2 * d

    def place(d):
        return n_z - 1 if d in (half_z, -half_z) else pos(d)

    def hops(way, e):
        return half_z if (way == 1) == (e == 0) else half_z - 1

    def send(src, dst, send_sem, recv_sem, device):
        return pltpu.make_async_remote_copy(
            src_ref=src,
            dst_ref=dst,
            send_sem=send_sem,
            recv_sem=recv_sem,
            device_id=device,
            device_id_type=MESH,
        )

    def run(fn, low, high):
        def body(i, carry):
            fn(i)
            return carry

        lax.fori_loop(low, high, body, 0)

    def lanes(i, n):
        return pl.ds(pl.multiple_of(i * n, n), n)

    loads = [
        pltpu.make_async_copy(src, dst, w_sem.at[i])
        for i, (src, dst) in enumerate(
            (
                (value_hbm, loc_vg.at[0]),
                (glu_hbm, loc_vg.at[1]),
                (ow_hbm, loc_o),
                (gate_hbm, gate_v),
                (up_hbm, up_v),
                (down_hbm, down_v),
                (mix_hbm, mix_v),
            )
        )
    ]
    for load in loads:
        load.start()

    barrier = pltpu.get_barrier_semaphore()

    def greet(device):
        pl.semaphore_signal(barrier, inc=1, device_id=device, device_id_type=MESH)

    run(lambda i: greet(((ep + i) % n_ep, tp)), 1, n_ep)
    run(lambda i: greet((ep, 2 * ((z + i) % n_z) + core)), 1, n_z)
    for device in ((ep, mate_tp), line_next, line_prev):
        greet(device)

    experts = 2 * n_ep
    eye = iota((tokens, tokens), 0) == iota((tokens, tokens), 1)

    def upright(row):
        return jnp.sum(jnp.where(eye, row, 0.0), axis=1, keepdims=True)

    chosen = [route_ref[k : k + 1, :] for k in range(2)]
    named = [(c == iota((experts, tokens), 0)).astype(F32) for c in chosen]
    earlier = (iota((tokens, tokens), 0) < iota((tokens, tokens), 1)).astype(F32)
    before = mm((named[0] + named[1]).astype(BF16), earlier.astype(BF16))
    spot_row = [
        (c // 2) * 16
        + (c % 2) * CAPS
        + jnp.sum(before * n, axis=0, keepdims=True).astype(jnp.int32)
        for c, n in zip(chosen, named)
    ]
    normed = rms_scale(x_ref[...], fgain_ref[...]).astype(BF16)
    picked = jnp.zeros((slots, half), F32)
    for h in range(2):
        at = iota((slots, tokens), 0) - 8 * h
        hit = jnp.logical_or(at == spot_row[0], at == spot_row[1])
        picked = picked + mm(
            jnp.where(hit, 1.0, 0.0).astype(BF16), normed[:, h * half : (h + 1) * half]
        )
    slab[...] = picked.astype(BF16).reshape(n_ep, 16, half)
    pl.semaphore_wait(barrier, n_ep - 1 + n_z - 1 + 3)

    def exchange(src, dst, send_sem, recv_sem):
        def copy(i):
            peer = (ep + i) % n_ep
            return send(
                src.at[peer], dst.at[ep], send_sem.at[i], recv_sem.at[i], (peer, tp)
            )

        return copy

    out_copy = exchange(slab, arrived, a_send, a_recv)
    run(lambda i: out_copy(i).start(), 1, n_ep)

    piece = [major[i] * n_s + minor[i] for i in range(2)]

    def vg_at(i, zs, who, at, count):
        return vg_all.at[i, zs, who, :, pl.ds(pl.multiple_of(at * unit, unit), count * unit)]

    def o_at(i, zs, who, at, count):
        return o_all.at[
            i, zs, pl.ds(pl.multiple_of(at * o_unit, o_unit), count * o_unit), lanes(who, 128)
        ]

    def column_copies(dz):
        device = (ep, 2 * ((z + dz) % n_z) + core)
        copies = []
        for i in range(2):
            copies.append(
                send(
                    loc_vg.at[i, :, lanes(piece[i], unit)],
                    vg_at(i, z, core, piece[i], 1),
                    c_send.at[dz, 2 * i],
                    c_recv.at[dz, 2 * i],
                    device,
                )
            )
            copies.append(
                send(
                    loc_o.at[i, lanes(piece[i], o_unit), :],
                    o_at(i, z, core, piece[i], 1),
                    c_send.at[dz, 2 * i + 1],
                    c_recv.at[dz, 2 * i + 1],
                    device,
                )
            )
        return copies

    own_copies = []
    for i in range(2):
        own_copies.append(
            pltpu.make_async_copy(
                loc_vg.at[i, :, lanes(piece[i], unit)],
                vg_at(i, z, core, piece[i], 1),
                h_sem.at[2 * i],
            )
        )
        own_copies.append(
            pltpu.make_async_copy(
                loc_o.at[i, lanes(piece[i], o_unit), :],
                o_at(i, z, core, piece[i], 1),
                h_sem.at[2 * i + 1],
            )
        )
    for load in loads[:3]:
        load.wait()

    def column_start(dz):
        for copy in column_copies(dz):
            copy.start()

    run(column_start, 1, n_z)
    for copy in own_copies:
        copy.start()
    arrived[ep] = slab[ep]

    def plane(i, phase, way, step):
        a, b = major[i], minor[i]
        zs = pl.ds(0, n_z) if step == 0 else pl.ds(0 if way == 1 else half_z, half_z)
        if phase == 0:
            source = (b + n_s - way * step) % n_s
            at, count = a * n_s + source, 1
            there = (a, (b + n_s + way) % n_s)
        else:
            source = (a + n_s - way * step) % n_s
            at, count = source * n_s, n_s
            there = ((a + n_s + way) % n_s, b)
        device = (there[0] * n_s + there[1] if i == 0 else there[1] * n_s + there[0], tp)
        mark = 2 * step + side[way]
        vg, o = vg_at(i, zs, core, at, count), o_at(i, zs, core, at, count)
        return [
            send(
                ref,
                ref,
                p_send.at[i, phase, 2 * mark + n],
                p_recv.at[i, phase, 2 * mark + n],
                device,
            )
            for n, ref in enumerate((vg, o))
        ]

    def plane_mate(i, turn):
        shift = (0, n_s - 1, 1, 2)[turn]
        at = ((major[i] + shift) % n_s) * n_s
        zs = pl.ds(0, n_z)
        return [
            send(ref, ref, t_send.at[i, turn, n], t_recv.at[i, turn, n], (ep, mate_tp))
            for n, ref in enumerate((vg_at(i, zs, core, at, n_s), o_at(i, zs, core, at, n_s)))
        ]

    def start(copies):
        for copy in copies:
            copy.start()

    def landed(copies):
        for copy in copies:
            copy.wait_recv()

    def left(copies):
        for copy in copies:
            copy.wait_send()

    run(lambda i: out_copy(i).wait_recv(), 1, n_ep)

    def to_rows(e, h, shape, row_dim, slot_dim):
        row, slot = iota(shape, row_dim), iota(shape, slot_dim)
        inner = slot % 8 - CAPS * e
        hit = (row == (slot // 16) * CAPS + inner) & ((slot // 8) % 2 == h)
        hit = hit & (inner >= 0) & (inner < CAPS)
        return jnp.where(hit, 1.0, 0.0).astype(BF16)

    def ring(way, e, k):
        return send(
            rows.at[e, place(-way * (k - 1)), 0],
            rows.at[e, place(-way * k), 0],
            g_send.at[side[way], e, k - 1],
            g_recv.at[side[way], e, k - 1],
            (ep, toward[way]),
        )

    def to_mate(e, p):
        return send(
            rows.at[e, p, 0], rows.at[e, p, 1], m_send.at[e, p], m_recv.at[e, p], (ep, mate_tp)
        )

    def part_to_mate(e, p):
        return send(
            parts.at[e, p, 1], mate.at[e, p], q_send.at[e, p], q_recv.at[e, p], (ep, mate_tp)
        )

    def ring_sum(way, e, k):
        return send(
            parts.at[e, place(way * k), 0],
            ring_in.at[side[way], e, k - 1],
            s_send.at[side[way], e, k - 1],
            s_recv.at[side[way], e, k - 1],
            (ep, toward[way]),
        )

    block = arrived[...].reshape(slots, half)
    for e in range(2):
        for h in range(2):
            rows[e, 0, 0, :, h * half : (h + 1) * half] = mm(
                to_rows(e, h, (cap, slots), 0, 1), block
            ).astype(BF16)
        for way in (1, -1):
            if hops(way, e) > 0:
                ring(way, e, 1).start()
        to_mate(e, 0).start()

    def column_landed(dz):
        landed(column_copies(dz))

    run(column_landed, 1, n_z)
    for copy in own_copies:
        copy.wait()
    for i in range(2):
        for way in (1, -1):
            start(plane(i, 0, way, 0))
    for load in loads[3:]:
        load.wait()

    def ffn(low, high):
        for e in range(2):
            for p in range(low, high):
                to_mate(e, p).wait_recv()
        count = (high - low) * 2 * cap

        def one(e):
            block = rows[e, low:high].reshape(count, width)
            gate = jnp.minimum(mm(block, gate_v[e]), CLAMP_LIMIT)
            up = jnp.clip(mm(block, up_v[e]), -CLAMP_LIMIT, CLAMP_LIMIT)
            hidden = ((up + 1.0) * gate * jax.nn.sigmoid(SWISH_ALPHA * gate)).astype(BF16)
            parts[e, low:high] = (
                mm(hidden, down_v[e]).astype(BF16).reshape(high - low, 2, cap, width)
            )

        run(one, 0, 2)
        for e in range(2):
            for p in range(low, high):
                part_to_mate(e, p).start()

    def chip_sum(low, high):
        for e in range(2):
            for p in range(low, high):
                part_to_mate(e, p).wait_recv()

        def add(p):
            for e in range(2):
                parts[e, p, 0] = (
                    parts[e, p, 0].astype(F32) + mate[e, p].astype(F32)
                ).astype(BF16)

        run(add, low, high)

    def plane_forward(phase):
        for i in range(2):
            for way in (1, -1):
                landed(plane(i, phase, way, 0))
                start(plane(i, phase, way, 1))

    def plane_done(phase):
        for i in range(2):
            for way in (1, -1):
                landed(plane(i, phase, way, 1))

    def gather_step(k):
        for e in range(2):
            for way in (1, -1):
                if k <= hops(way, e):
                    ring(way, e, k).wait_recv()
                    if k < hops(way, e):
                        ring(way, e, k + 1).start()
                    to_mate(e, place(-way * k)).start()

    def phase_two():
        plane_done(0)
        for i in range(2):
            for way in (1, -1):
                start(plane(i, 1, way, 0))
            start(plane_mate(i, 0))

    def norm_mix(i):
        at = pl.ds(pl.multiple_of(i * 16, 16), 16)
        normed_v[at, :] = rms_scale(mix_v[at, :], pgain_ref[...]).astype(BF16)

    def nt(a, b):
        return lax.dot_general(a, b, (((1,), (1,)), ((), ())), preferred_element_type=F32)

    rim_size = rim.shape[1]

    def glu(i):
        a = normed_v[...]
        value = nt(a, vg_all[0, i].reshape(128, width))
        gate = nt(a, vg_all[1, i].reshape(128, width))
        gated = (value * jax.nn.sigmoid(gate)).astype(BF16)
        ext[i, pl.ds(rim_size, length), :] = gated.astype(F32)
        tail_rows[i] = gated[length - rim_size :]

    rim_copy = send(tail_rows, rim, o_sem.at[0], o_sem.at[1], line_next)
    taps = taps_ref.shape[0]
    lead = rim_size - (taps - 1)
    blocks = 2
    span = length // blocks
    first = (ep + tp) == 0

    def conv(n):
        i, at = n // blocks, (n % blocks) * span
        acc = jnp.zeros((span, 128), F32)
        for r in range(8):
            picks = [j for j in range(taps) if (j + lead) % 8 == r]
            reach = max((j + lead) // 8 for j in picks) * 8
            moved = ext[i, pl.ds(at + r, span + reach), :]
            for j in picks:
                q = (j + lead) // 8 * 8
                acc = acc + taps_ref[j : j + 1, lanes(i, 128)] * moved[q : q + span]
        conv_v[pl.ds(pl.multiple_of(at, 8), span), lanes(i, 128)] = acc

    def activate(i):
        at = pl.ds(pl.multiple_of(i * 16, 16), 16)
        c = conv_v[at, :]
        c = c - jnp.mean(c, axis=-1, keepdims=True)
        var = jnp.mean(c * c, axis=-1, keepdims=True)
        c = c * lax.rsqrt(var + LAYER_EPSILON) * cgain_ref[...]
        act_v[at, :] = (c * jax.nn.sigmoid(c)).astype(BF16)

    def project(i):
        mid = act_v.shape[1] // 2
        proj_v[:, lanes(i, 256)] = mm(act_v[:, :mid], o_all[0, i]) + mm(
            act_v[:, mid:], o_all[1, i]
        )

    def norm_out(i):
        at = pl.ds(pl.multiple_of(i * 16, 16), 16)
        mixed_v[at, :] = rms_scale(proj_v[at, :], mgain_ref[...]).astype(BF16)

    def mixer_glu():
        for i in range(2):
            landed(plane_mate(i, 0))
            landed(plane_mate(i, 1))
            landed(plane_mate(i, 2))
            landed(plane_mate(i, 3))
        run(glu, 0, n_z)
        rim_copy.start()

    def mixer_conv():
        rim_copy.wait_recv()
        ext[:, :rim_size, :] = jnp.where(first, 0.0, rim[...].astype(F32))
        run(conv, 0, n_z * blocks)
        run(activate, 0, length // 16)

    mixed_copy = pltpu.make_async_copy(mixed_v, mixed_hbm, o_sem.at[2])

    def mixer_out():
        run(project, 0, n_z)
        run(norm_out, 0, length // 16)
        mixed_copy.start()

    ffn(0, 1)
    plane_forward(0)
    for k in range(1, half_z + 1):
        gather_step(k)
        if k < half_z:
            ffn(2 * k - 1, 2 * k + 1)
            if k == 1:
                phase_two()
                run(norm_mix, 0, length // 16)
            if k == half_z - 1:
                chip_sum(0, 2 * k + 1)
                for e in range(2):
                    for way in (1, -1):
                        if hops(way, e) == k:
                            ring_sum(way, e, k).start()
                plane_forward(1)
        else:
            ffn(n_z - 1, n_z)
            chip_sum(n_z - 1, n_z)

    for k in range(half_z, 0, -1):
        for e in range(2):
            for way in (1, -1):
                if k < hops(way, e):
                    ring_sum(way, e, k + 1).wait_recv()
                    p = place(way * k)
                    parts[e, p, 0] = (
                        parts[e, p, 0].astype(F32)
                        + ring_in[side[way], e, k].astype(F32)
                    ).astype(BF16)
                    ring_sum(way, e, k).start()
                elif k == half_z and hops(way, e) == k:
                    ring_sum(way, e, k).start()
        if k == half_z:
            for i in range(2):
                start(plane_mate(i, 1))
                start(plane_mate(i, 2))
            plane_done(1)
            for i in range(2):
                start(plane_mate(i, 3))
        if k == half_z - 1:
            mixer_glu()
        if k == half_z - 2:
            mixer_conv()
        if k == 1:
            mixer_out()
    done = []
    for e in range(2):
        total = parts[e, 0, 0].astype(F32)
        for way in (1, -1):
            if hops(way, e) > 0:
                ring_sum(way, e, 1).wait_recv()
                total = total + ring_in[side[way], e, 0].astype(F32)
        done.append(total.astype(BF16))

    back_rows = jnp.zeros((slots, half), F32)
    for e in range(2):
        for h in range(2):
            back_rows = back_rows + mm(
                to_rows(e, h, (slots, cap), 1, 0), done[e][:, h * half : (h + 1) * half]
            )
    back_slab[...] = back_rows.astype(BF16).reshape(n_ep, 16, half)
    back_copy = exchange(back_slab, back, b_send, b_recv)
    run(lambda i: back_copy(i).start(), 1, n_ep)
    back[ep] = back_slab[ep]
    mixes = []
    spot = [upright(s.astype(F32)).astype(jnp.int32) for s in spot_row]
    share_of = [upright(rw_ref[k : k + 1, :]) for k in range(2)]
    for h in range(2):
        at = iota((tokens, slots), 1) - 8 * h
        share = jnp.zeros((tokens, slots), F32)
        for k in range(2):
            share = share + jnp.where(at == spot[k], share_of[k], 0.0)
        high = share.astype(BF16)
        mixes.append((high, (share - high.astype(F32)).astype(BF16)))

    run(lambda i: out_copy(i).wait_send(), 1, n_ep)
    run(lambda dz: left(column_copies(dz)), 1, n_z)
    for i in range(2):
        for phase in range(2):
            for way in (1, -1):
                left(plane(i, phase, way, 0))
                left(plane(i, phase, way, 1))
        for turn in range(4):
            left(plane_mate(i, turn))
    for e in range(2):
        for way in (1, -1):
            for k in range(1, hops(way, e) + 1):
                ring(way, e, k).wait_send()
                ring_sum(way, e, k).wait_send()
        for p in range(n_z):
            to_mate(e, p).wait_send()
            part_to_mate(e, p).wait_send()
    rim_copy.wait_send()
    mixed_copy.wait()

    run(lambda i: back_copy(i).wait_recv(), 1, n_ep)
    results = back[...].reshape(slots, half)
    combined = [mm(high, results) + mm(low, results) for high, low in mixes]
    square = sum(jnp.sum(c * c, axis=1, keepdims=True) for c in combined)
    scale = lax.rsqrt(square / width + RMS_EPSILON)
    for h in range(2):
        cols = slice(h * half, (h + 1) * half)
        out_ref[:, cols] = (combined[h] * scale * egain_ref[:, cols]).astype(BF16)
    run(lambda i: back_copy(i).wait_send(), 1, n_ep)


def on_device(
    mixer_in,
    pre_gain,
    glu_value,
    glu_gate,
    conv_kernel,
    chan_gain,
    out_weight,
    mix_gain,
    expert_in,
    ffn_gain,
    routing,
    route_weight,
    gate_proj,
    up_proj,
    down_proj,
    expert_gain,
):
    n_ep, n_z = lax.axis_size("ep"), lax.axis_size("tp") // 2
    half_z = n_z // 2
    tokens, width = expert_in.shape
    length = mixer_in.shape[0]
    half, cap, hid = width // 2, n_ep * CAPS, gate_proj.shape[2]
    channels, cols = conv_kernel.shape[1], glu_value.shape[1]
    wide = out_weight.shape[1]
    rim_size = 32
    dma = pltpu.SemaphoreType.DMA
    vmem = pl.BlockSpec(memory_space=pltpu.VMEM)
    hbm = pl.BlockSpec(memory_space=pl.ANY)
    routed, mixed = pl.pallas_call(
        functools.partial(both_kernel, n_ep, n_z),
        out_shape=(
            jax.ShapeDtypeStruct((tokens, width), BF16),
            jax.ShapeDtypeStruct((length, width), BF16),
        ),
        in_specs=[vmem] * 9 + [hbm] * 7,
        out_specs=(vmem, hbm),
        scratch_shapes=[
            pltpu.VMEM((2, width, hid), BF16),
            pltpu.VMEM((2, width, hid), BF16),
            pltpu.VMEM((2, hid, width), BF16),
            pltpu.VMEM((length, width), BF16),
            pltpu.VMEM((2, cols, width), BF16),
            pltpu.VMEM((2, channels // 2, wide), BF16),
            pltpu.VMEM((n_ep, 16, half), BF16),
            pltpu.VMEM((n_ep, 16, half), BF16),
            pltpu.VMEM((2, n_z, 2, cap, width), BF16),
            pltpu.VMEM((2, n_z, 2, cap, width), BF16),
            pltpu.VMEM((2, n_z, cap, width), BF16),
            pltpu.VMEM((2, 2, half_z, cap, width), BF16),
            pltpu.VMEM((n_ep, 16, half), BF16),
            pltpu.VMEM((n_ep, 16, half), BF16),
            pltpu.VMEM((2, n_z, 2, cols, width), BF16),
            pltpu.VMEM((2, n_z, channels // 2, 2 * wide), BF16),
            pltpu.VMEM((length, width), BF16),
            pltpu.VMEM((n_z, rim_size + length, 2 * cols), F32),
            pltpu.VMEM((n_z, rim_size, 2 * cols), BF16),
            pltpu.VMEM((n_z, rim_size, 2 * cols), BF16),
            pltpu.VMEM((length, channels), F32),
            pltpu.VMEM((length, channels), BF16),
            pltpu.VMEM((length, width), F32),
            pltpu.VMEM((length, width), BF16),
            dma((7,)),
            dma((n_ep,)),
            dma((n_ep,)),
            dma((2, 2, half_z)),
            dma((2, 2, half_z)),
            dma((2, n_z)),
            dma((2, n_z)),
            dma((2, n_z)),
            dma((2, n_z)),
            dma((2, 2, half_z)),
            dma((2, 2, half_z)),
            dma((n_ep,)),
            dma((n_ep,)),
            dma((n_z, 4)),
            dma((n_z, 4)),
            dma((2, 2, 8)),
            dma((2, 2, 8)),
            dma((2, 4, 2)),
            dma((2, 4, 2)),
            dma((4,)),
            dma((3,)),
        ],
        compiler_params=pltpu.CompilerParams(
            collective_id=0, has_side_effects=True, vmem_limit_bytes=62 * 1024 * 1024
        ),
        name="both_modules",
    )(
        expert_in,
        ffn_gain.reshape(1, -1),
        routing.T,
        route_weight.T,
        expert_gain.reshape(1, -1),
        pre_gain.reshape(1, -1),
        conv_kernel,
        chan_gain.reshape(1, -1),
        mix_gain.reshape(1, -1),
        gate_proj,
        up_proj,
        down_proj,
        mixer_in,
        glu_value.T,
        glu_gate.T,
        out_weight.reshape(2, channels // 2, wide),
    )
    return (mixed, routed)


def solution(mesh):
    in_specs = (
        P(("ep", "tp"), None),
        P(),
        P(None, "tp"),
        P(None, "tp"),
        P(),
        P(),
        P(None, "tp"),
        P(),
        P(("ep", "tp"), None),
        P(),
        P(("ep", "tp"), None),
        P(("ep", "tp"), None),
        P("ep", None, "tp"),
        P("ep", None, "tp"),
        P("ep", "tp", None),
        P(),
    )
    out_specs = (P(("ep", "tp"), None), P(("ep", "tp"), None))
    return jax.shard_map(
        on_device, mesh=mesh, in_specs=in_specs, out_specs=out_specs, check_vma=False
    )
```

time: 232 us -> 111 us (0.48); the launches traced: 228 us -> 111 us
  local copies, waits for them, and re-layouts: 59 us -> 3 us
  waiting for transfers between devices: 28.7 us -> 0 us
  other arithmetic: 17.3 us -> 0 us
  between operations: 14.3 us -> 0.65 us
  Pallas kernels: 99.5 us -> 107 us
  matrix products: 7.37 us -> 0 us
    transpose x4 -> x0, local copies, waits for them, and re-layouts: 30.8 us -> none  [the longest x2 24.1 us: on_device(): full[:, :, :rows_v].transpose(0, 2, 1, 3).reshape(width, n_tp * 2 * cols)]
    all_gather x1 -> x0, waiting for transfers between devices: 28.7 us -> none  [on_device(): full = lax.all_gather(piece, ('ep', 'tp'), axis=0, tiled=False)]
    reduce_sum x3 -> x0, other arithmetic: 14.7 us -> none  [the longest x1 14.2 us: on_device(): row_mean = jnp.mean(conv_sum, axis=-1, keepdims=True)]
    unnamed x26 -> x4, local copies, waits for them, and re-layouts: 15.7 us -> 3 us
    dot_general x1 -> x0, local copies, waits for them, and re-layouts: 12.3 us -> none  [mm(): return jnp.dot(a, b, preferred_element_type=F32)]
    pallas_call x1, Pallas kernels: 99.5 us -> 107 us  [on_device(): pl.pallas_call(functools.partial(both_kernel, n_ep, n_z), out_shape=(jax....]
    dot_general x2 -> x0, matrix products: 7.37 us -> none  [mm(): return jnp.dot(a, b, preferred_element_type=F32)]
  transfers between devices with their start and end apart: 2 -> 0, of which waited for: 1 -> 0; matrix products, arithmetic and copies ran while one was open for 4% -> 0% of each run, Pallas kernels for 44% -> 0%
where the time goes in v2:
time: 111 us
  Pallas kernels  107 us (96%)
  local copies, waits for them, and re-layouts  3 us (3%)
    pallas_call x1, Pallas kernels, on_device(): pl.pallas_call(functools.partial(both_kernel, n_ep, n_z), out_shape=(jax....  107 us
    unnamed x4, local copies, waits for them, and re-layouts  3 us

profile of v2, /device:TPU:1, one launch (start us, length us, event | category | flops | bytes accessed | tf_op | source)
XLA Modules:
  0.0 110.9 jit_solution(5608723790883079655)
XLA Ops:
  0.6 107.3 %both_modules.1 = (bf16[32,2048]{1,0:T(8,128)(2,1)}, bf16[256,2048]{1,0:T(8,128)(2,1)}) custom-call(bf16[32,2048]{1,0:T(8,128)(2,1)} %x_ref.1, f32[1,2048]{1,0:T(1,128)} %bitcast.13, s32[2,32]{1,0:T(2,128)} %bitcast.18, f32[2,32]{1,0:T(2,128)} %bitcast.19, f32[1,2048]{1,0:T(1,128)} %bitcast.14, f32[1,2048]{1,0:T(1,128)} %bitcast.15, f32[31,1024]{1,0:T(8,128)} %taps_ref.1, ...), custom_call_target="tpu_custom_call" | custom-call | tf_op jit(solution)/shard_map/both_modules/pallas_call | solution.py:662
  107.9 0.0 copy-start
  107.9 2.3 %copy.20 = bf16[256,2048]{1,0:T(8,128)(2,1)} copy(bf16[256,2048]{1,0:T(8,128)(2,1)} %get-tuple-element.8) | data formatting | bytes 2097152
  110.3 0.0 copy-done
  110.3 0.7 copy.21
Async XLA Ops:
  107.9 2.4 %copy-start = (bf16[32,2048]{1,0:T(8,128)(2,1)S(1)}, bf16[32,2048]{1,0:T(8,128)(2,1)}, u32[]{:S(2)}) copy-start(bf16[32,2048]{1,0:T(8,128)(2,1)} %get-tuple-element.9) | copy-start | bytes 393220

commit v3 on v2

v3 whole, which is shorter than its diff:
```python
import functools

import jax
import jax.numpy as jnp
from jax import lax
from jax.experimental import pallas as pl
from jax.experimental.pallas import tpu as pltpu
from jax.sharding import PartitionSpec as P

RMS_EPSILON = 1e-06
LAYER_EPSILON = 1e-05
CLAMP_LIMIT = 7.0
SWISH_ALPHA = 1.702
CAPS = 3
MESH = pl.DeviceIdType.MESH
F32 = jnp.float32
BF16 = jnp.bfloat16


def iota(shape, dim):
    return lax.broadcasted_iota(jnp.int32, shape, dim)


def mm(a, b):
    return jnp.dot(a, b, preferred_element_type=F32)


def rms_scale(values, gain_row):
    values = values.astype(F32)
    return (
        values
        * lax.rsqrt(jnp.mean(values * values, axis=-1, keepdims=True) + RMS_EPSILON)
        * gain_row
    )


def both_kernel(
    n_ep,
    n_z,
    x_ref,
    fgain_ref,
    route_ref,
    rw_ref,
    egain_ref,
    pgain_ref,
    taps_ref,
    cgain_ref,
    gate_hbm,
    up_hbm,
    down_hbm,
    mix_hbm,
    value_hbm,
    glu_hbm,
    ow_hbm,
    out_ref,
    mixed_hbm,
    gate_v,
    up_v,
    down_v,
    mix_v,
    loc_vg,
    loc_o,
    slab,
    arrived,
    rows,
    parts,
    mate,
    ring_in,
    back_slab,
    back,
    vg_all,
    o_all,
    normed_v,
    ext,
    conv_v,
    act_v,
    proj_v,
    mixed_v,
    w_sem,
    a_send,
    a_recv,
    g_send,
    g_recv,
    m_send,
    m_recv,
    q_send,
    q_recv,
    s_send,
    s_recv,
    b_send,
    b_recv,
    c_send,
    c_recv,
    p_send,
    p_recv,
    t_send,
    t_recv,
    h_sem,
    o_sem,
):
    half_z = n_z // 2
    n_s = 4
    tokens, width = x_ref.shape
    cap = n_ep * CAPS
    slots = n_ep * 16
    parts_n = 8
    part_w = width // parts_n
    length = mix_hbm.shape[0]
    rim_size = mix_v.shape[0] - length
    unit = width // n_ep
    o_unit = loc_o.shape[1] // n_ep
    ep, tp = lax.axis_index("ep"), lax.axis_index("tp")
    z, core = tp // 2, tp % 2
    mate_tp = 2 * z + 1 - core
    next_tp = 2 * ((z + 1) % n_z) + core
    prev_tp = 2 * ((z + n_z - 1) % n_z) + core
    toward = {1: next_tp, -1: prev_tp}
    side = {1: 0, -1: 1}
    major = (ep // n_s, ep % n_s)
    minor = (ep % n_s, ep // n_s)
    after = (tp + 1) // (2 * n_z)
    line_next = ((ep + after) % n_ep, (tp + 1) % (2 * n_z))
    behind = (2 * n_z - tp) // (2 * n_z)
    line_prev = ((ep + n_ep - behind) % n_ep, (tp + 2 * n_z - 1) % (2 * n_z))

    def pos(d):
        return 2 * d - 1 if d > 0 else -2 * d

    def place(d):
        return n_z - 1 if d in (half_z, -half_z) else pos(d)

    def cols_of(way, k):
        if k < half_z:
            return slice(0, width)
        return pl.ds(side[way] * (width // 2), width // 2)

    def send(src, dst, send_sem, recv_sem, device):
        return pltpu.make_async_remote_copy(
            src_ref=src,
            dst_ref=dst,
            send_sem=send_sem,
            recv_sem=recv_sem,
            device_id=device,
            device_id_type=MESH,
        )

    def bulk(ref, send_sem, recv_sem):
        return send(ref, ref, send_sem, recv_sem, (ep, mate_tp))

    def run(fn, low, high, unroll=1):
        def body(i, carry):
            fn(i)
            return carry

        lax.fori_loop(low, high, body, 0, unroll=unroll)

    def lanes(i, n):
        return pl.ds(pl.multiple_of(i * n, n), n)

    loads = [
        pltpu.make_async_copy(src, dst, w_sem.at[i])
        for i, (src, dst) in enumerate(
            (
                (value_hbm, loc_vg.at[0]),
                (glu_hbm, loc_vg.at[1]),
                (ow_hbm, loc_o),
                (gate_hbm, gate_v),
                (up_hbm, up_v),
                (down_hbm, down_v),
                (mix_hbm, mix_v.at[rim_size:]),
            )
        )
    ]
    for load in loads:
        load.start()

    barrier = pltpu.get_barrier_semaphore()

    def greet(device):
        pl.semaphore_signal(barrier, inc=1, device_id=device, device_id_type=MESH)

    run(lambda i: greet(((ep + i) % n_ep, tp)), 1, n_ep)
    run(lambda i: greet((ep, 2 * ((z + i) % n_z) + core)), 1, n_z)
    for device in ((ep, mate_tp), line_next, line_prev):
        greet(device)

    experts = 2 * n_ep
    eye = iota((tokens, tokens), 0) == iota((tokens, tokens), 1)

    def upright(row):
        return jnp.sum(jnp.where(eye, row, 0.0), axis=1, keepdims=True)

    chosen = [route_ref[k : k + 1, :] for k in range(2)]
    named = [(c == iota((experts, tokens), 0)).astype(F32) for c in chosen]
    earlier = (iota((tokens, tokens), 0) < iota((tokens, tokens), 1)).astype(F32)
    before = mm((named[0] + named[1]).astype(BF16), earlier.astype(BF16))
    code_row = jnp.concatenate(
        [
            c.astype(F32) * 4.0 + jnp.sum(before * n, axis=0, keepdims=True)
            for c, n in zip(chosen, named)
        ],
        axis=0,
    )
    spread = (iota((tokens, parts_n * tokens), 1) % tokens) == iota(
        (tokens, parts_n * tokens), 0
    )
    code_wide = mm(code_row.astype(BF16), spread.astype(F32).astype(BF16))
    normed = rms_scale(x_ref[...], fgain_ref[...]).astype(BF16)
    stacked = jnp.concatenate(
        [normed[:, c * part_w : (c + 1) * part_w] for c in range(parts_n)], axis=0
    )
    shape = (slots, parts_n * tokens)
    same_part = iota(shape, 0) % parts_n == iota(shape, 1) // tokens
    for slot in range(CAPS):
        key = (iota(shape, 0) // parts_n * 4 + slot).astype(F32)
        hit = (code_wide[0:1] == key) | (code_wide[1:2] == key)
        picked = mm(jnp.where(hit & same_part, 1.0, 0.0).astype(BF16), stacked)
        slab[:, :, slot * part_w : (slot + 1) * part_w] = picked.astype(BF16).reshape(
            n_ep, 16, part_w
        )
    pl.semaphore_wait(barrier, n_ep - 1 + n_z - 1 + 3)

    def exchange(src, dst, send_sem, recv_sem):
        def copy(i):
            peer = (ep + i) % n_ep
            return send(
                src.at[peer], dst.at[ep], send_sem.at[0], recv_sem.at[0], (peer, tp)
            )

        return copy

    rim_copy = send(
        mix_hbm.at[length - rim_size :],
        mix_v.at[:rim_size],
        o_sem.at[0],
        o_sem.at[1],
        line_next,
    )
    rim_copy.start()
    out_copy = exchange(slab, arrived, a_send, a_recv)
    run(lambda i: out_copy(i).start(), 1, n_ep)

    piece = [major[i] * n_s + minor[i] for i in range(2)]

    def vg_at(i, zs, who, at, count):
        return vg_all.at[zs, i, who, :, pl.ds(pl.multiple_of(at * unit, unit), count * unit)]

    def o_at(i, zs, who, at, count):
        return o_all.at[
            i, zs, pl.ds(pl.multiple_of(at * o_unit, o_unit), count * o_unit), lanes(who, 128)
        ]

    def column_copies(dz):
        device = (ep, 2 * ((z + dz) % n_z) + core)
        copies = []
        for i in range(2):
            copies.append(
                send(
                    loc_vg.at[i, :, lanes(piece[i], unit)],
                    vg_at(i, z, core, piece[i], 1),
                    c_send.at[0],
                    c_recv.at[0],
                    device,
                )
            )
            copies.append(
                send(
                    loc_o.at[i, lanes(piece[i], o_unit), :],
                    o_at(i, z, core, piece[i], 1),
                    c_send.at[1],
                    c_recv.at[1],
                    device,
                )
            )
        return copies

    own_copies = []
    for i in range(2):
        own_copies.append(
            pltpu.make_async_copy(
                loc_vg.at[i, :, lanes(piece[i], unit)],
                vg_at(i, z, core, piece[i], 1),
                h_sem.at[2 * i],
            )
        )
        own_copies.append(
            pltpu.make_async_copy(
                loc_o.at[i, lanes(piece[i], o_unit), :],
                o_at(i, z, core, piece[i], 1),
                h_sem.at[2 * i + 1],
            )
        )
    for load in loads[:3]:
        load.wait()

    def column_start(dz):
        for copy in column_copies(dz):
            copy.start()

    run(column_start, 1, n_z)
    for copy in own_copies:
        copy.start()
    arrived[ep] = slab[ep]

    def plane(i, phase, way, step):
        a, b = major[i], minor[i]
        zs = pl.ds(0, n_z) if step == 0 else pl.ds(0 if way == 1 else half_z, half_z)
        if phase == 0:
            source = (b + n_s - way * step) % n_s
            at, count = a * n_s + source, 1
            there = (a, (b + n_s + way) % n_s)
        else:
            source = (a + n_s - way * step) % n_s
            at, count = source * n_s, n_s
            there = ((a + n_s + way) % n_s, b)
        device = (there[0] * n_s + there[1] if i == 0 else there[1] * n_s + there[0], tp)
        mark = 2 * step + side[way]
        vg, o = vg_at(i, zs, core, at, count), o_at(i, zs, core, at, count)
        return [
            send(
                ref,
                ref,
                p_send.at[n],
                p_recv.at[i, phase, 2 * mark + n],
                device,
            )
            for n, ref in enumerate((vg, o))
        ]

    def plane_mate(i, turn):
        shift = (0, n_s - 1, 1, 2)[turn]
        at = ((major[i] + shift) % n_s) * n_s
        zs = pl.ds(0, n_z)
        return [
            send(ref, ref, t_send.at[n], t_recv.at[i, turn, n], (ep, mate_tp))
            for n, ref in enumerate((vg_at(i, zs, core, at, n_s), o_at(i, zs, core, at, n_s)))
        ]

    def start(copies):
        for copy in copies:
            copy.start()

    def landed(copies):
        for copy in copies:
            copy.wait_recv()

    def left(copies):
        for copy in copies:
            copy.wait_send()

    bulk(arrived.at[1:], a_send.at[0], a_recv.at[0]).wait_recv()

    def turned(across):
        turn = iota((slots, slots), 1 - across)
        hit = iota((slots, slots), across) == turn % n_ep * 16 + turn // n_ep
        return jnp.where(hit, 1.0, 0.0).astype(BF16)

    def ring(way, e, k):
        cols = cols_of(way, k)
        return send(
            rows.at[e, place(-way * (k - 1)), 0, :, cols],
            rows.at[e, place(-way * k), 0, :, cols],
            g_send.at[0],
            g_recv.at[side[way], e, k - 1],
            (ep, toward[way]),
        )

    def to_mate(e, p):
        return send(
            rows.at[e, p, 0], rows.at[e, p, 1], m_send.at[0], m_recv.at[e, p], (ep, mate_tp)
        )

    def part_to_mate(e, p):
        return send(
            parts.at[e, p, 1], mate.at[e, p], q_send.at[0], q_recv.at[e, p], (ep, mate_tp)
        )

    def ring_sum(way, e, k):
        cols = cols_of(way, k)
        return send(
            parts.at[e, place(way * k), 0, :, cols],
            ring_in.at[side[way], e, k - 1, :, cols],
            s_send.at[0],
            s_recv.at[side[way], e, k - 1],
            (ep, toward[way]),
        )

    block = arrived[...].reshape(slots, CAPS * part_w)
    block = mm(turned(1), block).astype(BF16)
    for e in range(2):
        for c in range(parts_n):
            at = (e * parts_n + c) * n_ep
            for slot in range(CAPS):
                rows[
                    e, 0, 0, slot * n_ep : (slot + 1) * n_ep, c * part_w : (c + 1) * part_w
                ] = block[at : at + n_ep, slot * part_w : (slot + 1) * part_w]
        if e == 0:
            for way in (1, -1):
                ring(way, e, 1).start()
        to_mate(e, 0).start()

    column_bulk = [
        bulk(loc_vg.at[:, :, : (n_z - 1) * unit], c_send.at[0], c_recv.at[0]),
        bulk(loc_o.at[:, : (n_z - 1) * o_unit, :], c_send.at[1], c_recv.at[1]),
    ]

    def columns_in():
        landed(column_bulk)
        for copy in own_copies:
            copy.wait()
        for i in range(2):
            for way in (1, -1):
                start(plane(i, 0, way, 0))

    for load in loads[3:]:
        load.wait()

    def ffn(e, low, high):
        for p in range(low, high):
            to_mate(e, p).wait_recv()
        count = (high - low) * 2 * cap
        block = rows[e, low:high].reshape(count, width)
        gate = jnp.minimum(mm(block, gate_v[e]), CLAMP_LIMIT)
        up = jnp.clip(mm(block, up_v[e]), -CLAMP_LIMIT, CLAMP_LIMIT)
        hidden = ((up + 1.0) * gate * jax.nn.sigmoid(SWISH_ALPHA * gate)).astype(BF16)
        parts[e, low:high] = (
            mm(hidden, down_v[e]).astype(BF16).reshape(high - low, 2, cap, width)
        )
        for p in range(low, high):
            part_to_mate(e, p).start()

    def chip_sum(e, low, high):
        for p in range(low, high):
            part_to_mate(e, p).wait_recv()

        def add(p):
            parts[e, p, 0] = (
                parts[e, p, 0].astype(F32) + mate[e, p].astype(F32)
            ).astype(BF16)

        run(add, low, high)

    def plane_forward(phase, i):
        for way in (1, -1):
            landed(plane(i, phase, way, 0))
            start(plane(i, phase, way, 1))
        if phase == 1:
            start(plane_mate(i, 1))
            start(plane_mate(i, 2))

    def phase_two(i):
        for way in (1, -1):
            landed(plane(i, 0, way, 1))
        for way in (1, -1):
            start(plane(i, 1, way, 0))
        start(plane_mate(i, 0))

    def gather_step(e, k, way):
        ring(way, e, k).wait_recv()
        if k < half_z:
            ring(way, e, k + 1).start()
            to_mate(e, place(-way * k)).start()

    def gather_far(e):
        for way in (1, -1):
            gather_step(e, half_z, way)
        to_mate(e, place(half_z)).start()

    def scatter_first(e):
        for way in (1, -1):
            ring_sum(way, e, half_z).start()

    def scatter_step(e, k, way):
        ring_sum(way, e, k + 1).wait_recv()
        p, cols = place(way * k), cols_of(way, k + 1)
        parts[e, p, 0, :, cols] = (
            parts[e, p, 0, :, cols].astype(F32)
            + ring_in[side[way], e, k, :, cols].astype(F32)
        ).astype(BF16)
        ring_sum(way, e, k).start()

    def scatter_last(e):
        total = parts[e, 0, 0].astype(F32)
        for way in (1, -1):
            ring_sum(way, e, 1).wait_recv()
            total = total + ring_in[side[way], e, 0].astype(F32)
        return total.astype(BF16)

    def norm_mix(i):
        at = pl.ds(pl.multiple_of(i * 16, 16), 16)
        normed_v[at, :] = rms_scale(mix_v[at, :], pgain_ref[...]).astype(BF16)

    def nt(a, b):
        return lax.dot_general(a, b, (((1,), (1,)), ((), ())), preferred_element_type=F32)

    def glu(i):
        a = normed_v[...]
        pre = nt(a, vg_all[i].reshape(256, width))
        gated = (pre[:, :128] * jax.nn.sigmoid(pre[:, 128:])).astype(BF16).astype(F32)
        ext[i] = jnp.where(real, gated, 0.0)

    taps = taps_ref.shape[0]
    lead = rim_size - (taps - 1)
    blocks = 2
    span = length // blocks
    real = iota((rim_size + length, 128), 0) >= jnp.where((ep + tp) == 0, rim_size, 0)

    def conv(n):
        i, at = n // blocks, (n % blocks) * span
        acc = jnp.zeros((span, 128), F32)
        for r in range(8):
            picks = [j for j in range(taps) if (j + lead) % 8 == r]
            reach = max((j + lead) // 8 for j in picks) * 8
            moved = ext[i, pl.ds(at + r, span + reach), :]
            for j in picks:
                q = (j + lead) // 8 * 8
                acc = acc + taps_ref[j : j + 1, lanes(i, 128)] * moved[q : q + span]
        conv_v[pl.ds(pl.multiple_of(at, 8), span), lanes(i, 128)] = acc

    def activate(i):
        at = pl.ds(pl.multiple_of(i * 32, 32), 32)
        c = conv_v[at, :]
        c = c - jnp.mean(c, axis=-1, keepdims=True)
        var = jnp.mean(c * c, axis=-1, keepdims=True)
        c = c * lax.rsqrt(var + LAYER_EPSILON) * cgain_ref[...]
        act_v[at, :] = (c * jax.nn.sigmoid(c)).astype(BF16)

    def project(i):
        mid = act_v.shape[1] // 2
        proj_v[:, lanes(i, 256)] = mm(act_v[:, :mid], o_all[0, i]) + mm(
            act_v[:, mid:], o_all[1, i]
        )

    def norm_out(i):
        at = pl.ds(pl.multiple_of(i * 16, 16), 16)
        mixed_v[at, :] = rms_scale(proj_v[at, :], 1.0).astype(BF16)

    def weights_out(i):
        for way in (1, -1):
            landed(plane(i, 1, way, 1))
        start(plane_mate(i, 3))

    def weights_in():
        for i in range(2):
            for turn in range(4):
                landed(plane_mate(i, turn))

    def mixer_glu(low, high):
        run(glu, low, high)

    def mixer_conv(low, high):
        run(conv, low, high)

    def mixer_act():
        run(activate, 0, length // 32, 2)

    mixed_copy = pltpu.make_async_copy(mixed_v, mixed_hbm, o_sem.at[2])

    def norm_mix_all():
        rim_copy.wait_recv()
        run(norm_mix, 0, (rim_size + length) // 16, 2)

    def mixer_out():
        run(project, 0, n_z)
        run(norm_out, 0, length // 16, 2)
        mixed_copy.start()

    ffn(0, 0, 1)
    columns_in()
    norm_mix_all()
    for way in (1, -1):
        ring(way, 1, 1).start()
    gather_step(0, 1, -1)
    gather_step(0, 1, 1)
    ffn(1, 0, 1)
    plane_forward(0, 0)
    plane_forward(0, 1)
    gather_step(1, 1, 1)
    gather_step(1, 1, -1)
    gather_step(0, 2, -1)
    gather_step(0, 2, 1)
    phase_two(0)
    phase_two(1)
    ffn(0, 1, 3)
    gather_step(1, 2, -1)
    gather_step(1, 2, 1)
    ffn(1, 1, 3)
    chip_sum(0, 0, 3)
    gather_step(0, 3, 1)
    gather_step(0, 3, -1)
    ffn(0, 3, 5)
    chip_sum(1, 0, 3)
    ffn(1, 3, 5)
    gather_step(1, 3, -1)
    gather_step(1, 3, 1)
    ffn(0, 5, 7)
    gather_far(0)
    chip_sum(0, 3, 5)
    chip_sum(1, 3, 5)
    ffn(0, 7, 8)
    chip_sum(0, 5, 7)
    gather_far(1)
    ffn(1, 5, 7)
    chip_sum(0, 7, 8)
    scatter_first(0)
    ffn(1, 7, 8)
    plane_forward(1, 0)
    plane_forward(1, 1)
    chip_sum(1, 5, 7)
    chip_sum(1, 7, 8)
    scatter_first(1)

    scatter_step(0, 3, 1)
    scatter_step(0, 3, -1)
    scatter_step(1, 3, -1)
    scatter_step(1, 3, 1)
    scatter_step(0, 2, -1)
    scatter_step(0, 2, 1)
    weights_out(0)
    weights_out(1)
    scatter_step(1, 2, -1)
    scatter_step(1, 2, 1)
    weights_in()
    mixer_glu(0, 6)
    scatter_step(0, 1, 1)
    scatter_step(0, 1, -1)
    mixer_glu(6, n_z)
    scatter_step(1, 1, 1)
    scatter_step(1, 1, -1)
    mixer_conv(0, n_z * blocks)
    done = [scatter_last(0), None]
    mixer_act()
    done[1] = scatter_last(1)

    gathered = jnp.concatenate(
        [
            jnp.concatenate(
                [
                    done[e][slot * n_ep : (slot + 1) * n_ep, c * part_w : (c + 1) * part_w]
                    for slot in range(CAPS)
                ],
                axis=1,
            )
            for e in range(2)
            for c in range(parts_n)
        ],
        axis=0,
    )
    back_slab[...] = mm(turned(0), gathered).astype(BF16).reshape(n_ep, 16, CAPS * part_w)
    back_copy = exchange(back_slab, back, b_send, b_recv)
    run(lambda i: back_copy(i).start(), 1, n_ep)
    back[ep] = back_slab[ep]
    mixer_out()
    code = [upright(code_row[k : k + 1, :]) for k in range(2)]
    share_of = [upright(rw_ref[k : k + 1, :]) for k in range(2)]
    code, share_of = (
        [jnp.concatenate([c] * parts_n, axis=0) for c in cs] for cs in (code, share_of)
    )
    shape = (parts_n * tokens, slots)
    same_part = iota(shape, 1) % parts_n == iota(shape, 0) // tokens
    mixes = []
    for slot in range(CAPS):
        key = (iota(shape, 1) // parts_n * 4 + slot).astype(F32)
        share = jnp.zeros(shape, F32)
        for k in range(2):
            share = share + jnp.where((code[k] == key) & same_part, share_of[k], 0.0)
        high = share.astype(BF16)
        mixes.append((high, (share - high.astype(F32)).astype(BF16)))

    once = [
        (arrived.at[1:], a_send.at[0]),
        (loc_vg.at[:, :, : (n_z - 1) * unit], c_send.at[0]),
        (loc_o.at[:, : (n_z - 1) * o_unit, :], c_send.at[1]),
        (vg_all.at[:, :, 0, :, : 15 * unit], p_send.at[0]),
        (o_all.at[:, :, : 15 * o_unit, :128], p_send.at[1]),
        (vg_all.at[:, :, 0], t_send.at[0]),
        (o_all.at[:, :, :, :128], t_send.at[1]),
        (rows.at[:, : n_z - 1, 0], g_send.at[0]),
        (parts.at[:, : n_z - 1, 0], s_send.at[0]),
        (rows.at[:, :, 0], m_send.at[0]),
        (parts.at[:, :, 1], q_send.at[0]),
    ]
    for ref, sem in once:
        bulk(ref, sem, o_sem.at[1]).wait_send()
    rim_copy.wait_send()
    mixed_copy.wait()

    bulk(back.at[1:], b_send.at[0], b_recv.at[0]).wait_recv()
    results = back[...].reshape(slots, CAPS * part_w)
    combined = jnp.zeros((parts_n * tokens, part_w), F32)
    for slot, (high, low) in enumerate(mixes):
        part = results[:, slot * part_w : (slot + 1) * part_w]
        combined = combined + mm(high, part) + mm(low, part)
    square = jnp.sum(combined * combined, axis=1, keepdims=True)
    square = sum(square[c * tokens : (c + 1) * tokens] for c in range(parts_n))
    scale = lax.rsqrt(square / width + RMS_EPSILON)
    for c in range(parts_n):
        cols = slice(c * part_w, (c + 1) * part_w)
        out_ref[:, cols] = (
            combined[c * tokens : (c + 1) * tokens] * scale * egain_ref[:, cols]
        ).astype(BF16)
    bulk(back.at[1:], b_send.at[0], b_recv.at[0]).wait_send()


def on_device(
    mixer_in,
    pre_gain,
    glu_value,
    glu_gate,
    conv_kernel,
    chan_gain,
    out_weight,
    mix_gain,
    expert_in,
    ffn_gain,
    routing,
    route_weight,
    gate_proj,
    up_proj,
    down_proj,
    expert_gain,
):
    n_ep, n_z = lax.axis_size("ep"), lax.axis_size("tp") // 2
    half_z = n_z // 2
    tokens, width = expert_in.shape
    length = mixer_in.shape[0]
    slab_w, cap, hid = CAPS * (width // 8), n_ep * CAPS, gate_proj.shape[2]
    channels, cols = conv_kernel.shape[1], glu_value.shape[1]
    wide = out_weight.shape[1]
    rim_size = 32
    dma = pltpu.SemaphoreType.DMA
    vmem = pl.BlockSpec(memory_space=pltpu.VMEM)
    hbm = pl.BlockSpec(memory_space=pl.ANY)
    routed, mixed = pl.pallas_call(
        functools.partial(both_kernel, n_ep, n_z),
        out_shape=(
            jax.ShapeDtypeStruct((tokens, width), BF16),
            jax.ShapeDtypeStruct((length, width), BF16),
        ),
        in_specs=[vmem] * 8 + [hbm] * 7,
        out_specs=(vmem, hbm),
        scratch_shapes=[
            pltpu.VMEM((2, width, hid), BF16),
            pltpu.VMEM((2, width, hid), BF16),
            pltpu.VMEM((2, hid, width), BF16),
            pltpu.VMEM((rim_size + length, width), BF16),
            pltpu.VMEM((2, cols, width), BF16),
            pltpu.VMEM((2, channels // 2, wide), BF16),
            pltpu.VMEM((n_ep, 16, slab_w), BF16),
            pltpu.VMEM((n_ep, 16, slab_w), BF16),
            pltpu.VMEM((2, n_z, 2, cap, width), BF16),
            pltpu.VMEM((2, n_z, 2, cap, width), BF16),
            pltpu.VMEM((2, n_z, cap, width), BF16),
            pltpu.VMEM((2, 2, half_z, cap, width), BF16),
            pltpu.VMEM((n_ep, 16, slab_w), BF16),
            pltpu.VMEM((n_ep, 16, slab_w), BF16),
            pltpu.VMEM((n_z, 2, 2, cols, width), BF16),
            pltpu.VMEM((2, n_z, channels // 2, 2 * wide), BF16),
            pltpu.VMEM((rim_size + length, width), BF16),
            pltpu.VMEM((n_z, rim_size + length, 2 * cols), F32),
            pltpu.VMEM((length, channels), F32),
            pltpu.VMEM((length, channels), BF16),
            pltpu.VMEM((length, width), F32),
            pltpu.VMEM((length, width), BF16),
            dma((7,)),
            dma((1,)),
            dma((1,)),
            dma((1,)),
            dma((2, 2, half_z)),
            dma((1,)),
            dma((2, n_z)),
            dma((1,)),
            dma((2, n_z)),
            dma((1,)),
            dma((2, 2, half_z)),
            dma((1,)),
            dma((1,)),
            dma((2,)),
            dma((2,)),
            dma((2,)),
            dma((2, 2, 8)),
            dma((2,)),
            dma((2, 4, 2)),
            dma((4,)),
            dma((3,)),
        ],
        compiler_params=pltpu.CompilerParams(
            collective_id=0, has_side_effects=True, vmem_limit_bytes=62 * 1024 * 1024
        ),
        name="both_modules",
    )(
        expert_in,
        ffn_gain.reshape(1, -1),
        routing.T,
        route_weight.T,
        expert_gain.reshape(1, -1),
        pre_gain.reshape(1, -1),
        conv_kernel,
        chan_gain.reshape(1, -1),
        gate_proj,
        up_proj,
        down_proj,
        mixer_in,
        glu_value.T,
        glu_gate.T,
        out_weight.reshape(2, channels // 2, wide),
    )
    return ((mixed.astype(F32) * mix_gain).astype(BF16), routed)


def solution(mesh):
    in_specs = (
        P(("ep", "tp"), None),
        P(),
        P(None, "tp"),
        P(None, "tp"),
        P(),
        P(),
        P(None, "tp"),
        P(),
        P(("ep", "tp"), None),
        P(),
        P(("ep", "tp"), None),
        P(("ep", "tp"), None),
        P("ep", None, "tp"),
        P("ep", None, "tp"),
        P("ep", "tp", None),
        P(),
    )
    out_specs = (P(("ep", "tp"), None), P(("ep", "tp"), None))
    return jax.shard_map(
        on_device, mesh=mesh, in_specs=in_specs, out_specs=out_specs, check_vma=False
    )
```

time: 111 us -> 98.8 us (0.89)
  Pallas kernels: 107 us -> 94.6 us
  other arithmetic: 0 us -> 2.46 us
  local copies, waits for them, and re-layouts: 3 us -> 0.66 us
    pallas_call x1, Pallas kernels: 107 us -> 94.6 us  [on_device(): pl.pallas_call(functools.partial(both_kernel, n_ep, n_z), out_shape=(jax....]
    convert_element_type x0 -> x1, other arithmetic: none -> 2.46 us  [on_device(): return ((mixed.astype(F32) * mix_gain).astype(BF16), routed)]
    unnamed x4 -> x5, local copies, waits for them, and re-layouts: 3 us -> 0.66 us
where the time goes in v3:
time: 98.8 us; the launch traced here: 98.4 us
  Pallas kernels  94.6 us (96%)
  other arithmetic  2.46 us (2%)
    pallas_call x1, Pallas kernels, on_device(): pl.pallas_call(functools.partial(both_kernel, n_ep, n_z), out_shape=(jax....  94.6 us
    convert_element_type x1, other arithmetic, on_device(): return ((mixed.astype(F32) * mix_gain).astype(BF16), routed)  2.46 us

profile of v3, /device:TPU:1, one launch (start us, length us, event | category | flops | bytes accessed | tf_op | source)
XLA Modules:
  0.0 98.4 jit_solution(1195492386813638992)
XLA Ops:
  0.6 0.0 copy-start.1
  0.6 94.6 %both_modules.1 = (bf16[32,2048]{1,0:T(8,128)(2,1)}, bf16[256,2048]{1,0:T(8,128)(2,1)}) custom-call(bf16[32,2048]{1,0:T(8,128)(2,1)} %x_ref.1, f32[1,2048]{1,0:T(1,128)} %bitcast.12, s32[2,32]{1,0:T(2,128)} %bitcast.16, f32[2,32]{1,0:T(2,128)} %bitcast.17, f32[1,2048]{1,0:T(1,128)} %bitcast.13, f32[1,2048]{1,0:T(1,128)} %bitcast.14, f32[31,1024]{1,0:T(8,128)} %taps_ref.1, ...), custom_call_target="tpu_custom_call" | custom-call | tf_op jit(solution)/shard_map/both_modules/pallas_call | solution.py:734
  95.3 0.0 copy-start
  95.3 0.0 copy-done.1
  95.3 2.5 %multiply_convert_fusion = bf16[256,2048]{1,0:T(8,128)(2,1)} fusion(bf16[256,2048]{1,0:T(8,128)(2,1)} %get-tuple-element.4, f32[2048]{0:T(1024)S(1)} %copy-done.1), kind=kLoop, calls=%fused_computation | loop fusion | flops 1572864 | bytes 2105344 | tf_op jit(solution)/shard_map/convert_element_type | solution.py:808
  97.7 0.0 copy-done
  97.7 0.7 copy.19
Async XLA Ops:
  0.6 94.6 %copy-start.1 = (f32[2048]{0:T(1024)S(1)}, f32[2048]{0:T(1024)}, u32[]{:S(2)}) copy-start(f32[2048]{0:T(1024)} %param.23) | copy-start | bytes 24580
  95.3 2.5 %copy-start = (bf16[32,2048]{1,0:T(8,128)(2,1)S(1)}, bf16[32,2048]{1,0:T(8,128)(2,1)}, u32[]{:S(2)}) copy-start(bf16[32,2048]{1,0:T(8,128)(2,1)} %get-tuple-element.9) | copy-start | bytes 393220

commit v4 on v3

--- a/solution.py
+++ b/solution.py
@@ -53,7 +53,7 @@
     glu_hbm,
     ow_hbm,
     out_ref,
-    mixed_hbm,
+    mixed_ref,
     gate_v,
     up_v,
     down_v,
@@ -75,7 +75,6 @@
     conv_v,
     act_v,
     proj_v,
-    mixed_v,
     w_sem,
     a_send,
     a_recv,
@@ -250,59 +249,40 @@
             i, zs, pl.ds(pl.multiple_of(at * o_unit, o_unit), count * o_unit), lanes(who, 128)
         ]
 
-    def column_copies(dz):
-        device = (ep, 2 * ((z + dz) % n_z) + core)
-        copies = []
+    def piece_from(i, n):
+        if n == 0:
+            return loc_vg.at[i, :, lanes(piece[i], unit)]
+        return loc_o.at[i, lanes(piece[i], o_unit), :]
+
+    def region(i, zs, at, count, n):
+        return vg_at(i, zs, core, at, count) if n == 0 else o_at(i, zs, core, at, count)
+
+    def own_copy(i, n):
+        return pltpu.make_async_copy(
+            piece_from(i, n), region(i, z, piece[i], 1, n), h_sem.at[2 * i + n]
+        )
+
+    def column_send(n):
+        def one(dz):
+            for i in range(2):
+                send(
+                    piece_from(i, n),
+                    region(i, z, piece[i], 1, n),
+                    c_send.at[n],
+                    c_recv.at[n],
+                    (ep, 2 * ((z + dz) % n_z) + core),
+                ).start()
+
+        run(one, 1, n_z)
         for i in range(2):
-            copies.append(
-                send(
-                    loc_vg.at[i, :, lanes(piece[i], unit)],
-                    vg_at(i, z, core, piece[i], 1),
-                    c_send.at[0],
-                    c_recv.at[0],
-                    device,
-                )
-            )
-            copies.append(
-                send(
-                    loc_o.at[i, lanes(piece[i], o_unit), :],
-                    o_at(i, z, core, piece[i], 1),
-                    c_send.at[1],
-                    c_recv.at[1],
-                    device,
-                )
-            )
-        return copies
-
-    own_copies = []
-    for i in range(2):
-        own_copies.append(
-            pltpu.make_async_copy(
-                loc_vg.at[i, :, lanes(piece[i], unit)],
-                vg_at(i, z, core, piece[i], 1),
-                h_sem.at[2 * i],
-            )
-        )
-        own_copies.append(
-            pltpu.make_async_copy(
-                loc_o.at[i, lanes(piece[i], o_unit), :],
-                o_at(i, z, core, piece[i], 1),
-                h_sem.at[2 * i + 1],
-            )
-        )
-    for load in loads[:3]:
+            own_copy(i, n).start()
+
+    for load in loads[:2]:
         load.wait()
-
-    def column_start(dz):
-        for copy in column_copies(dz):
-            copy.start()
-
-    run(column_start, 1, n_z)
-    for copy in own_copies:
-        copy.start()
+    column_send(0)
     arrived[ep] = slab[ep]
 
-    def plane(i, phase, way, step):
+    def plane(i, phase, way, step, n):
         a, b = major[i], minor[i]
         zs = pl.ds(0, n_z) if step == 0 else pl.ds(0 if way == 1 else half_z, half_z)
         if phase == 0:
@@ -313,40 +293,20 @@
             source = (a + n_s - way * step) % n_s
             at, count = source * n_s, n_s
             there = ((a + n_s + way) % n_s, b)
-        device = (there[0] * n_s + there[1] if i == 0 else there[1] * n_s + there[0], tp)
-        mark = 2 * step + side[way]
-        vg, o = vg_at(i, zs, core, at, count), o_at(i, zs, core, at, count)
-        return [
-            send(
-                ref,
-                ref,
-                p_send.at[n],
-                p_recv.at[i, phase, 2 * mark + n],
-                device,
-            )
-            for n, ref in enumerate((vg, o))
-        ]
-
-    def plane_mate(i, turn):
+        ref = region(i, zs, at, count, n)
+        return send(
+            ref,
+            ref,
+            p_send.at[n],
+            p_recv.at[i, phase, 2 * (2 * step + side[way]) + n],
+            (there[0] * n_s + there[1] if i == 0 else there[1] * n_s + there[0], tp),
+        )
+
+    def plane_mate(i, turn, n):
         shift = (0, n_s - 1, 1, 2)[turn]
         at = ((major[i] + shift) % n_s) * n_s
-        zs = pl.ds(0, n_z)
-        return [
-            send(ref, ref, t_send.at[n], t_recv.at[i, turn, n], (ep, mate_tp))
-            for n, ref in enumerate((vg_at(i, zs, core, at, n_s), o_at(i, zs, core, at, n_s)))
-        ]
-
-    def start(copies):
-        for copy in copies:
-            copy.start()
-
-    def landed(copies):
-        for copy in copies:
-            copy.wait_recv()
-
-    def left(copies):
-        for copy in copies:
-            copy.wait_send()
+        ref = region(i, pl.ds(0, n_z), at, n_s, n)
+        return send(ref, ref, t_send.at[n], t_recv.at[n], (ep, mate_tp))
 
     bulk(arrived.at[1:], a_send.at[0], a_recv.at[0]).wait_recv()
 
@@ -375,13 +335,16 @@
             parts.at[e, p, 1], mate.at[e, p], q_send.at[0], q_recv.at[e, p], (ep, mate_tp)
         )
 
-    def ring_sum(way, e, k):
-        cols = cols_of(way, k)
+    def ring_sum(way, e, k, early=False):
+        cols, mark = cols_of(way, k), k - 1
+        if k == half_z - 1:
+            cols = cols_of(-way if early else way, half_z)
+            mark = half_z if early else mark
         return send(
             parts.at[e, place(way * k), 0, :, cols],
             ring_in.at[side[way], e, k - 1, :, cols],
             s_send.at[0],
-            s_recv.at[side[way], e, k - 1],
+            s_recv.at[side[way], e, mark],
             (ep, toward[way]),
         )
 
@@ -404,15 +367,15 @@
         bulk(loc_o.at[:, : (n_z - 1) * o_unit, :], c_send.at[1], c_recv.at[1]),
     ]
 
-    def columns_in():
-        landed(column_bulk)
-        for copy in own_copies:
-            copy.wait()
+    def columns_in(n):
+        column_bulk[n].wait_recv()
+        for i in range(2):
+            own_copy(i, n).wait()
         for i in range(2):
             for way in (1, -1):
-                start(plane(i, 0, way, 0))
-
-    for load in loads[3:]:
+                plane(i, 0, way, 0, n).start()
+
+    for load in loads[2:]:
         load.wait()
 
     def ffn(e, low, high):
@@ -440,20 +403,30 @@
 
         run(add, low, high)
 
-    def plane_forward(phase, i):
-        for way in (1, -1):
-            landed(plane(i, phase, way, 0))
-            start(plane(i, phase, way, 1))
-        if phase == 1:
-            start(plane_mate(i, 1))
-            start(plane_mate(i, 2))
-
-    def phase_two(i):
-        for way in (1, -1):
-            landed(plane(i, 0, way, 1))
-        for way in (1, -1):
-            start(plane(i, 1, way, 0))
-        start(plane_mate(i, 0))
+    def plane_forward(phase, n):
+        for i in range(2):
+            for way in (1, -1):
+                plane(i, phase, way, 0, n).wait_recv()
+                plane(i, phase, way, 1, n).start()
+
+    def phase_two(n):
+        for i in range(2):
+            for way in (1, -1):
+                plane(i, 0, way, 1, n).wait_recv()
+            for way in (1, -1):
+                plane(i, 1, way, 0, n).start()
+            plane_mate(i, 0, n).start()
+
+    def weights_out(n):
+        for i in range(2):
+            for way in (1, -1):
+                plane(i, 1, way, 1, n).wait_recv()
+            plane_mate(i, 3, n).start()
+
+    def weights_mid(n):
+        for i in range(2):
+            for turn in (1, 2):
+                plane_mate(i, turn, n).start()
 
     def gather_step(e, k, way):
         ring(way, e, k).wait_recv()
@@ -470,8 +443,14 @@
         for way in (1, -1):
             ring_sum(way, e, half_z).start()
 
+    def scatter_early(e):
+        for way in (1, -1):
+            ring_sum(way, e, half_z - 1, True).start()
+
     def scatter_step(e, k, way):
         ring_sum(way, e, k + 1).wait_recv()
+        if k == half_z - 2:
+            ring_sum(way, e, k + 1, True).wait_recv()
         p, cols = place(way * k), cols_of(way, k + 1)
         parts[e, p, 0, :, cols] = (
             parts[e, p, 0, :, cols].astype(F32)
@@ -533,17 +512,11 @@
 
     def norm_out(i):
         at = pl.ds(pl.multiple_of(i * 16, 16), 16)
-        mixed_v[at, :] = rms_scale(proj_v[at, :], 1.0).astype(BF16)
-
-    def weights_out(i):
-        for way in (1, -1):
-            landed(plane(i, 1, way, 1))
-        start(plane_mate(i, 3))
-
-    def weights_in():
-        for i in range(2):
-            for turn in range(4):
-                landed(plane_mate(i, turn))
+        mixed_ref[at, :] = rms_scale(proj_v[at, :], 1.0).astype(BF16)
+
+    def weights_in(n):
+        ref = (vg_all.at[:, :, 0], o_all.at[:, :, :, :128])[n]
+        bulk(ref, t_send.at[n], t_recv.at[n]).wait_recv()
 
     def mixer_glu(low, high):
         run(glu, low, high)
@@ -553,20 +526,17 @@
 
     def mixer_act():
         run(activate, 0, length // 32, 2)
-
-    mixed_copy = pltpu.make_async_copy(mixed_v, mixed_hbm, o_sem.at[2])
 
     def norm_mix_all():
         rim_copy.wait_recv()
         run(norm_mix, 0, (rim_size + length) // 16, 2)
 
     def mixer_out():
-        run(project, 0, n_z)
+        run(project, n_z // 2, n_z)
         run(norm_out, 0, length // 16, 2)
-        mixed_copy.start()
 
     ffn(0, 0, 1)
-    columns_in()
+    columns_in(0)
     norm_mix_all()
     for way in (1, -1):
         ring(way, 1, 1).start()
@@ -574,13 +544,11 @@
     gather_step(0, 1, 1)
     ffn(1, 0, 1)
     plane_forward(0, 0)
-    plane_forward(0, 1)
     gather_step(1, 1, 1)
     gather_step(1, 1, -1)
     gather_step(0, 2, -1)
     gather_step(0, 2, 1)
     phase_two(0)
-    phase_two(1)
     ffn(0, 1, 3)
     gather_step(1, 2, -1)
     gather_step(1, 2, 1)
@@ -593,79 +561,104 @@
     ffn(1, 3, 5)
     gather_step(1, 3, -1)
     gather_step(1, 3, 1)
+    column_send(1)
     ffn(0, 5, 7)
+    ffn(1, 5, 7)
     gather_far(0)
+    chip_sum(0, 5, 7)
+    scatter_early(0)
+    plane_forward(1, 0)
     chip_sum(0, 3, 5)
     chip_sum(1, 3, 5)
     ffn(0, 7, 8)
-    chip_sum(0, 5, 7)
     gather_far(1)
-    ffn(1, 5, 7)
+    chip_sum(1, 5, 7)
     chip_sum(0, 7, 8)
     scatter_first(0)
+    scatter_early(1)
     ffn(1, 7, 8)
-    plane_forward(1, 0)
-    plane_forward(1, 1)
-    chip_sum(1, 5, 7)
     chip_sum(1, 7, 8)
     scatter_first(1)
+    weights_mid(0)
+    columns_in(1)
 
     scatter_step(0, 3, 1)
     scatter_step(0, 3, -1)
+    plane_forward(0, 1)
     scatter_step(1, 3, -1)
     scatter_step(1, 3, 1)
+    weights_out(0)
+    phase_two(1)
     scatter_step(0, 2, -1)
     scatter_step(0, 2, 1)
-    weights_out(0)
-    weights_out(1)
+    weights_in(0)
+    mixer_glu(0, 4)
     scatter_step(1, 2, -1)
     scatter_step(1, 2, 1)
-    weights_in()
-    mixer_glu(0, 6)
+    mixer_glu(4, n_z)
+    mixer_conv(0, n_z * blocks)
     scatter_step(0, 1, 1)
     scatter_step(0, 1, -1)
-    mixer_glu(6, n_z)
+    plane_forward(1, 1)
+    weights_mid(1)
+    mixer_act()
     scatter_step(1, 1, 1)
     scatter_step(1, 1, -1)
-    mixer_conv(0, n_z * blocks)
-    done = [scatter_last(0), None]
-    mixer_act()
-    done[1] = scatter_last(1)
-
-    gathered = jnp.concatenate(
-        [
-            jnp.concatenate(
-                [
-                    done[e][slot * n_ep : (slot + 1) * n_ep, c * part_w : (c + 1) * part_w]
-                    for slot in range(CAPS)
-                ],
-                axis=1,
-            )
-            for e in range(2)
-            for c in range(parts_n)
-        ],
-        axis=0,
-    )
-    back_slab[...] = mm(turned(0), gathered).astype(BF16).reshape(n_ep, 16, CAPS * part_w)
-    back_copy = exchange(back_slab, back, b_send, b_recv)
-    run(lambda i: back_copy(i).start(), 1, n_ep)
-    back[ep] = back_slab[ep]
+
+    group = n_ep * parts_n
+    turn = iota((group, group), 1)
+    hit = iota((group, group), 0) == turn % n_ep * parts_n + turn // n_ep
+    turn_back = jnp.where(hit, 1.0, 0.0).astype(BF16)
+
+    def back_copy(e, i):
+        peer = (ep + i) % n_ep
+        return send(
+            back_slab.at[e, peer], back.at[e, ep], b_send.at[e], b_recv.at[e], (peer, tp)
+        )
+
+    def send_back(e):
+        done = scatter_last(e)
+        gathered = jnp.concatenate(
+            [
+                jnp.concatenate(
+                    [
+                        done[slot * n_ep : (slot + 1) * n_ep, c * part_w : (c + 1) * part_w]
+                        for slot in range(CAPS)
+                    ],
+                    axis=1,
+                )
+                for c in range(parts_n)
+            ],
+            axis=0,
+        )
+        back_slab[e] = mm(turn_back, gathered).astype(BF16).reshape(
+            n_ep, parts_n, CAPS * part_w
+        )
+        run(lambda i: back_copy(e, i).start(), 1, n_ep)
+        back[e, ep] = back_slab[e, ep]
+
+    weights_out(1)
+    send_back(0)
+    weights_in(1)
+    run(project, 0, n_z // 2)
+    send_back(1)
     mixer_out()
     code = [upright(code_row[k : k + 1, :]) for k in range(2)]
     share_of = [upright(rw_ref[k : k + 1, :]) for k in range(2)]
     code, share_of = (
         [jnp.concatenate([c] * parts_n, axis=0) for c in cs] for cs in (code, share_of)
     )
-    shape = (parts_n * tokens, slots)
+    shape = (parts_n * tokens, group)
     same_part = iota(shape, 1) % parts_n == iota(shape, 0) // tokens
     mixes = []
-    for slot in range(CAPS):
-        key = (iota(shape, 1) // parts_n * 4 + slot).astype(F32)
-        share = jnp.zeros(shape, F32)
-        for k in range(2):
-            share = share + jnp.where((code[k] == key) & same_part, share_of[k], 0.0)
-        high = share.astype(BF16)
-        mixes.append((high, (share - high.astype(F32)).astype(BF16)))
+    for e in range(2):
+        for slot in range(CAPS):
+            key = (iota(shape, 1) // parts_n * 8 + 4 * e + slot).astype(F32)
+            share = jnp.zeros(shape, F32)
+            for k in range(2):
+                share = share + jnp.where((code[k] == key) & same_part, share_of[k], 0.0)
+            high = share.astype(BF16)
+            mixes.append((high, (share - high.astype(F32)).astype(BF16)))
 
     once = [
         (arrived.at[1:], a_send.at[0]),
@@ -683,14 +676,15 @@
     for ref, sem in once:
         bulk(ref, sem, o_sem.at[1]).wait_send()
     rim_copy.wait_send()
-    mixed_copy.wait()
-
-    bulk(back.at[1:], b_send.at[0], b_recv.at[0]).wait_recv()
-    results = back[...].reshape(slots, CAPS * part_w)
+
     combined = jnp.zeros((parts_n * tokens, part_w), F32)
-    for slot, (high, low) in enumerate(mixes):
-        part = results[:, slot * part_w : (slot + 1) * part_w]
-        combined = combined + mm(high, part) + mm(low, part)
+    for e in range(2):
+        bulk(back.at[e, 1:], b_send.at[e], b_recv.at[e]).wait_recv()
+        results = back[e].reshape(group, CAPS * part_w)
+        for slot in range(CAPS):
+            high, low = mixes[e * CAPS + slot]
+            part = results[:, slot * part_w : (slot + 1) * part_w]
+            combined = combined + mm(high, part) + mm(low, part)
     square = jnp.sum(combined * combined, axis=1, keepdims=True)
     square = sum(square[c * tokens : (c + 1) * tokens] for c in range(parts_n))
     scale = lax.rsqrt(square / width + RMS_EPSILON)
@@ -699,7 +693,8 @@
         out_ref[:, cols] = (
             combined[c * tokens : (c + 1) * tokens] * scale * egain_ref[:, cols]
         ).astype(BF16)
-    bulk(back.at[1:], b_send.at[0], b_recv.at[0]).wait_send()
+    for e in range(2):
+        bulk(back.at[e, 1:], b_send.at[e], b_recv.at[e]).wait_send()
 
 
 def on_device(
@@ -734,11 +729,11 @@
     routed, mixed = pl.pallas_call(
         functools.partial(both_kernel, n_ep, n_z),
         out_shape=(
-            jax.ShapeDtypeStruct((tokens, width), BF16),
-            jax.ShapeDtypeStruct((length, width), BF16),
+            pltpu.VMEM((tokens, width), BF16),
+            pltpu.VMEM((length, width), BF16),
         ),
         in_specs=[vmem] * 8 + [hbm] * 7,
-        out_specs=(vmem, hbm),
+        out_specs=(vmem, vmem),
         scratch_shapes=[
             pltpu.VMEM((2, width, hid), BF16),
             pltpu.VMEM((2, width, hid), BF16),
@@ -752,8 +747,8 @@
             pltpu.VMEM((2, n_z, 2, cap, width), BF16),
             pltpu.VMEM((2, n_z, cap, width), BF16),
             pltpu.VMEM((2, 2, half_z, cap, width), BF16),
-            pltpu.VMEM((n_ep, 16, slab_w), BF16),
-            pltpu.VMEM((n_ep, 16, slab_w), BF16),
+            pltpu.VMEM((2, n_ep, 8, slab_w), BF16),
+            pltpu.VMEM((2, n_ep, 8, slab_w), BF16),
             pltpu.VMEM((n_z, 2, 2, cols, width), BF16),
             pltpu.VMEM((2, n_z, channels // 2, 2 * wide), BF16),
             pltpu.VMEM((rim_size + length, width), BF16),
@@ -761,7 +756,6 @@
             pltpu.VMEM((length, channels), F32),
             pltpu.VMEM((length, channels), BF16),
             pltpu.VMEM((length, width), F32),
-            pltpu.VMEM((length, width), BF16),
             dma((7,)),
             dma((1,)),
             dma((1,)),
@@ -772,20 +766,20 @@
             dma((1,)),
             dma((2, n_z)),
             dma((1,)),
-            dma((2, 2, half_z)),
-            dma((1,)),
-            dma((1,)),
+            dma((2, 2, half_z + 1)),
+            dma((2,)),
+            dma((2,)),
             dma((2,)),
             dma((2,)),
             dma((2,)),
             dma((2, 2, 8)),
             dma((2,)),
-            dma((2, 4, 2)),
+            dma((2,)),
             dma((4,)),
-            dma((3,)),
+            dma((2,)),
         ],
         compiler_params=pltpu.CompilerParams(
-            collective_id=0, has_side_effects=True, vmem_limit_bytes=62 * 1024 * 1024
+            collective_id=0, has_side_effects=True, vmem_limit_bytes=60 * 1024 * 1024
         ),
         name="both_modules",
     )(

time: 98.8 us -> 92.9 us (0.940)
  Pallas kernels: 94.6 us -> 90.2 us
  other arithmetic: 2.46 us -> 1.19 us
    pallas_call x1, Pallas kernels: 94.6 us -> 90.2 us  [on_device(): pl.pallas_call(functools.partial(both_kernel, n_ep, n_z), out_shape=(pltp...]
    convert_element_type x1, other arithmetic: 2.46 us -> 1.19 us  [on_device(): return ((mixed.astype(F32) * mix_gain).astype(BF16), routed)]
where the time goes in v4:
time: 92.9 us; the launch traced here: 92.7 us
  Pallas kernels  90.2 us (97%)
  other arithmetic  1.19 us (1%)
    pallas_call x1, Pallas kernels, on_device(): pl.pallas_call(functools.partial(both_kernel, n_ep, n_z), out_shape=(pltp...  90.2 us

profile of v4, /device:TPU:1, one launch (start us, length us, event | category | flops | bytes accessed | tf_op | source)
XLA Modules:
  0.0 92.7 jit_solution(10044668505924475461)
XLA Ops:
  0.6 0.0 copy-start
  0.6 90.2 %both_modules.1 = (bf16[32,2048]{1,0:T(8,128)(2,1)S(1)}, bf16[256,2048]{1,0:T(8,128)(2,1)S(1)}) custom-call(bf16[32,2048]{1,0:T(8,128)(2,1)} %x_ref.1, f32[1,2048]{1,0:T(1,128)} %bitcast.12, s32[2,32]{1,0:T(2,128)} %bitcast.16, f32[2,32]{1,0:T(2,128)} %bitcast.17, f32[1,2048]{1,0:T(1,128)} %bitcast.13, f32[1,2048]{1,0:T(1,128)} %bitcast.14, ...), custom_call_target="tpu_custom_call" | custom-call | tf_op jit(solution)/shard_map/both_modules/pallas_call | solution.py:729
  90.8 0.0 copy-done
  90.8 1.2 %multiply_convert_fusion = bf16[256,2048]{1,0:T(8,128)(2,1)} fusion(bf16[256,2048]{1,0:T(8,128)(2,1)S(1)} %get-tuple-element.4, f32[2048]{0:T(1024)S(1)} %copy-done), kind=kLoop, calls=%fused_computation | loop fusion | flops 1572864 | bytes 2105344 | tf_op jit(solution)/shard_map/convert_element_type | solution.py:802
  92.0 0.7 copy.19
Async XLA Ops:
  0.6 90.2 %copy-start = (f32[2048]{0:T(1024)S(1)}, f32[2048]{0:T(1024)}, u32[]{:S(2)}) copy-start(f32[2048]{0:T(1024)} %param.23) | copy-start | bytes 24580

commit v5 on v4

--- a/solution.py
+++ b/solution.py
@@ -208,25 +208,30 @@
     stacked = jnp.concatenate(
         [normed[:, c * part_w : (c + 1) * part_w] for c in range(parts_n)], axis=0
     )
-    shape = (slots, parts_n * tokens)
+    group = n_ep * parts_n
+    shape = (group, parts_n * tokens)
     same_part = iota(shape, 0) % parts_n == iota(shape, 1) // tokens
-    for slot in range(CAPS):
-        key = (iota(shape, 0) // parts_n * 4 + slot).astype(F32)
-        hit = (code_wide[0:1] == key) | (code_wide[1:2] == key)
-        picked = mm(jnp.where(hit & same_part, 1.0, 0.0).astype(BF16), stacked)
-        slab[:, :, slot * part_w : (slot + 1) * part_w] = picked.astype(BF16).reshape(
-            n_ep, 16, part_w
-        )
+    for e in range(2):
+        for slot in range(CAPS):
+            key = (iota(shape, 0) // parts_n * 8 + 4 * e + slot).astype(F32)
+            hit = (code_wide[0:1] == key) | (code_wide[1:2] == key)
+            picked = mm(jnp.where(hit & same_part, 1.0, 0.0).astype(BF16), stacked)
+            slab[e, :, :, slot * part_w : (slot + 1) * part_w] = picked.astype(
+                BF16
+            ).reshape(n_ep, parts_n, part_w)
     pl.semaphore_wait(barrier, n_ep - 1 + n_z - 1 + 3)
 
-    def exchange(src, dst, send_sem, recv_sem):
-        def copy(i):
-            peer = (ep + i) % n_ep
-            return send(
-                src.at[peer], dst.at[ep], send_sem.at[0], recv_sem.at[0], (peer, tp)
-            )
-
-        return copy
+    offsets = sorted(
+        [(dy, dx) for dy in range(n_s) for dx in range(n_s) if dy or dx],
+        key=lambda d: -(min(d[0], n_s - d[0]) + min(d[1], n_s - d[1])),
+    )
+
+    def exchange(src, dst, send_sem, recv_sem, e):
+        for dy, dx in offsets:
+            peer = ((ep // n_s + dy) % n_s) * n_s + (ep % n_s + dx) % n_s
+            send(
+                src.at[e, peer], dst.at[e, ep], send_sem.at[e], recv_sem.at[e], (peer, tp)
+            ).start()
 
     rim_copy = send(
         mix_hbm.at[length - rim_size :],
@@ -235,9 +240,8 @@
         o_sem.at[1],
         line_next,
     )
-    rim_copy.start()
-    out_copy = exchange(slab, arrived, a_send, a_recv)
-    run(lambda i: out_copy(i).start(), 1, n_ep)
+    for e in range(2):
+        exchange(slab, arrived, a_send, a_recv, e)
 
     piece = [major[i] * n_s + minor[i] for i in range(2)]
 
@@ -280,7 +284,9 @@
     for load in loads[:2]:
         load.wait()
     column_send(0)
-    arrived[ep] = slab[ep]
+    rim_copy.start()
+    for e in range(2):
+        arrived[e, ep] = slab[e, ep]
 
     def plane(i, phase, way, step, n):
         a, b = major[i], minor[i]
@@ -308,11 +314,10 @@
         ref = region(i, pl.ds(0, n_z), at, n_s, n)
         return send(ref, ref, t_send.at[n], t_recv.at[n], (ep, mate_tp))
 
-    bulk(arrived.at[1:], a_send.at[0], a_recv.at[0]).wait_recv()
 
     def turned(across):
-        turn = iota((slots, slots), 1 - across)
-        hit = iota((slots, slots), across) == turn % n_ep * 16 + turn // n_ep
+        turn = iota((group, group), 1 - across)
+        hit = iota((group, group), across) == turn % n_ep * parts_n + turn // n_ep
         return jnp.where(hit, 1.0, 0.0).astype(BF16)
 
     def ring(way, e, k):
@@ -348,11 +353,13 @@
             (ep, toward[way]),
         )
 
-    block = arrived[...].reshape(slots, CAPS * part_w)
-    block = mm(turned(1), block).astype(BF16)
-    for e in range(2):
+    turn_in = turned(1)
+
+    def take_in(e):
+        bulk(arrived.at[e, 1:], a_send.at[e], a_recv.at[e]).wait_recv()
+        block = mm(turn_in, arrived[e].reshape(group, CAPS * part_w)).astype(BF16)
         for c in range(parts_n):
-            at = (e * parts_n + c) * n_ep
+            at = c * n_ep
             for slot in range(CAPS):
                 rows[
                     e, 0, 0, slot * n_ep : (slot + 1) * n_ep, c * part_w : (c + 1) * part_w
@@ -361,6 +368,9 @@
             for way in (1, -1):
                 ring(way, e, 1).start()
         to_mate(e, 0).start()
+
+    take_in(0)
+    take_in(1)
 
     column_bulk = [
         bulk(loc_vg.at[:, :, : (n_z - 1) * unit], c_send.at[0], c_recv.at[0]),
@@ -605,16 +615,7 @@
     scatter_step(1, 1, 1)
     scatter_step(1, 1, -1)
 
-    group = n_ep * parts_n
-    turn = iota((group, group), 1)
-    hit = iota((group, group), 0) == turn % n_ep * parts_n + turn // n_ep
-    turn_back = jnp.where(hit, 1.0, 0.0).astype(BF16)
-
-    def back_copy(e, i):
-        peer = (ep + i) % n_ep
-        return send(
-            back_slab.at[e, peer], back.at[e, ep], b_send.at[e], b_recv.at[e], (peer, tp)
-        )
+    turn_back = turned(0)
 
     def send_back(e):
         done = scatter_last(e)
@@ -634,7 +635,7 @@
         back_slab[e] = mm(turn_back, gathered).astype(BF16).reshape(
             n_ep, parts_n, CAPS * part_w
         )
-        run(lambda i: back_copy(e, i).start(), 1, n_ep)
+        exchange(back_slab, back, b_send, b_recv, e)
         back[e, ep] = back_slab[e, ep]
 
     weights_out(1)
@@ -661,7 +662,8 @@
             mixes.append((high, (share - high.astype(F32)).astype(BF16)))
 
     once = [
-        (arrived.at[1:], a_send.at[0]),
+        (arrived.at[0, 1:], a_send.at[0]),
+        (arrived.at[1, 1:], a_send.at[1]),
         (loc_vg.at[:, :, : (n_z - 1) * unit], c_send.at[0]),
         (loc_o.at[:, : (n_z - 1) * o_unit, :], c_send.at[1]),
         (vg_all.at[:, :, 0, :, : 15 * unit], p_send.at[0]),
@@ -741,8 +743,8 @@
             pltpu.VMEM((rim_size + length, width), BF16),
             pltpu.VMEM((2, cols, width), BF16),
             pltpu.VMEM((2, channels // 2, wide), BF16),
-            pltpu.VMEM((n_ep, 16, slab_w), BF16),
-            pltpu.VMEM((n_ep, 16, slab_w), BF16),
+            pltpu.VMEM((2, n_ep, 8, slab_w), BF16),
+            pltpu.VMEM((2, n_ep, 8, slab_w), BF16),
             pltpu.VMEM((2, n_z, 2, cap, width), BF16),
             pltpu.VMEM((2, n_z, 2, cap, width), BF16),
             pltpu.VMEM((2, n_z, cap, width), BF16),
@@ -757,8 +759,8 @@
             pltpu.VMEM((length, channels), BF16),
             pltpu.VMEM((length, width), F32),
             dma((7,)),
-            dma((1,)),
-            dma((1,)),
+            dma((2,)),
+            dma((2,)),
             dma((1,)),
             dma((2, 2, half_z)),
             dma((1,)),

time: 92.9 us -> 91 us (0.980)
  Pallas kernels: 90.2 us -> 88.4 us
    pallas_call x1, Pallas kernels: 90.2 us -> 88.4 us  [on_device(): pl.pallas_call(functools.partial(both_kernel, n_ep, n_z), out_shape=(pltp...]
where the time goes in v5:
time: 91 us; the launch traced here: 90.9 us
  Pallas kernels  88.4 us (97%)
  other arithmetic  1.19 us (1%)
    pallas_call x1, Pallas kernels, on_device(): pl.pallas_call(functools.partial(both_kernel, n_ep, n_z), out_shape=(pltp...  88.4 us

profile of v5, /device:TPU:1, one launch (start us, length us, event | category | flops | bytes accessed | tf_op | source)
XLA Modules:
  0.0 90.9 jit_solution(14035474291313635798)
XLA Ops:
  0.6 0.0 copy-start
  0.6 88.4 %both_modules.1 = (bf16[32,2048]{1,0:T(8,128)(2,1)S(1)}, bf16[256,2048]{1,0:T(8,128)(2,1)S(1)}) custom-call(bf16[32,2048]{1,0:T(8,128)(2,1)} %x_ref.1, f32[1,2048]{1,0:T(1,128)} %bitcast.12, s32[2,32]{1,0:T(2,128)} %bitcast.16, f32[2,32]{1,0:T(2,128)} %bitcast.17, f32[1,2048]{1,0:T(1,128)} %bitcast.13, f32[1,2048]{1,0:T(1,128)} %bitcast.14, ...), custom_call_target="tpu_custom_call" | custom-call | tf_op jit(solution)/shard_map/both_modules/pallas_call | solution.py:731
  89.0 0.0 copy-done
  89.0 1.2 %multiply_convert_fusion = bf16[256,2048]{1,0:T(8,128)(2,1)} fusion(bf16[256,2048]{1,0:T(8,128)(2,1)S(1)} %get-tuple-element.4, f32[2048]{0:T(1024)S(1)} %copy-done), kind=kLoop, calls=%fused_computation | loop fusion | flops 1572864 | bytes 2105344 | tf_op jit(solution)/shard_map/convert_element_type | solution.py:804
  90.2 0.7 copy.19
Async XLA Ops:
  0.6 88.4 %copy-start = (f32[2048]{0:T(1024)S(1)}, f32[2048]{0:T(1024)}, u32[]{:S(2)}) copy-start(f32[2048]{0:T(1024)} %param.23) | copy-start | bytes 24580

commit v6 on v5

--- a/solution.py
+++ b/solution.py
@@ -45,6 +45,7 @@
     pgain_ref,
     taps_ref,
     cgain_ref,
+    mgain_ref,
     gate_hbm,
     up_hbm,
     down_hbm,
@@ -522,7 +523,7 @@
 
     def norm_out(i):
         at = pl.ds(pl.multiple_of(i * 16, 16), 16)
-        mixed_ref[at, :] = rms_scale(proj_v[at, :], 1.0).astype(BF16)
+        mixed_ref[at, :] = rms_scale(proj_v[at, :], mgain_ref[...]).astype(BF16)
 
     def weights_in(n):
         ref = (vg_all.at[:, :, 0], o_all.at[:, :, :, :128])[n]
@@ -699,6 +700,20 @@
         bulk(back.at[e, 1:], b_send.at[e], b_recv.at[e]).wait_send()
 
 
+def write_results(mixed_ref, routed_ref, mixed_hbm, routed_hbm, sem):
+    rows = mixed_ref.shape[0] // 4
+    copies = [pltpu.make_async_copy(routed_ref, routed_hbm, sem.at[4])]
+    for i in range(4):
+        at = slice(i * rows, (i + 1) * rows)
+        copies.append(
+            pltpu.make_async_copy(mixed_ref.at[at, :], mixed_hbm.at[at, :], sem.at[i])
+        )
+    for copy in copies:
+        copy.start()
+    for copy in copies:
+        copy.wait()
+
+
 def on_device(
     mixer_in,
     pre_gain,
@@ -734,7 +749,7 @@
             pltpu.VMEM((tokens, width), BF16),
             pltpu.VMEM((length, width), BF16),
         ),
-        in_specs=[vmem] * 8 + [hbm] * 7,
+        in_specs=[vmem] * 9 + [hbm] * 7,
         out_specs=(vmem, vmem),
         scratch_shapes=[
             pltpu.VMEM((2, width, hid), BF16),
@@ -793,6 +808,7 @@
         pre_gain.reshape(1, -1),
         conv_kernel,
         chan_gain.reshape(1, -1),
+        mix_gain.reshape(1, -1),
         gate_proj,
         up_proj,
         down_proj,
@@ -801,7 +817,18 @@
         glu_gate.T,
         out_weight.reshape(2, channels // 2, wide),
     )
-    return ((mixed.astype(F32) * mix_gain).astype(BF16), routed)
+    return pl.pallas_call(
+        write_results,
+        out_shape=(
+            jax.ShapeDtypeStruct((length, width), BF16),
+            jax.ShapeDtypeStruct((tokens, width), BF16),
+        ),
+        in_specs=[vmem] * 2,
+        out_specs=(hbm, hbm),
+        scratch_shapes=[dma((5,))],
+        compiler_params=pltpu.CompilerParams(vmem_limit_bytes=4 * 1024 * 1024),
+        name="write_results",
+    )(mixed, routed)
 
 
 def solution(mesh):

time: 91 us -> 90.2 us (level)
  other arithmetic: 1.19 us -> 0 us
  Pallas kernels: 88.4 us -> 89.4 us
    convert_element_type x1 -> x0, other arithmetic: 1.19 us -> none  [on_device(): return ((mixed.astype(F32) * mix_gain).astype(BF16), routed)]
    pallas_call x0 -> x1, Pallas kernels: none -> 1.05 us  [on_device(): pl.pallas_call(write_results, out_shape=(jax.ShapeDtypeStruct((length, wi...]
where the time goes in v6:
time: 90.2 us; the launch traced here: 90.1 us
  Pallas kernels  89.4 us (99%)
    pallas_call x1, Pallas kernels, on_device(): pl.pallas_call(functools.partial(both_kernel, n_ep, n_z), out_shape=(pltp...  88.4 us

profile of v6, /device:TPU:1, one launch (start us, length us, event | category | flops | bytes accessed | tf_op | source)
XLA Modules:
  0.0 90.1 jit_solution(3479258608529754940)
XLA Ops:
  0.6 88.4 %both_modules.1 = (bf16[32,2048]{1,0:T(8,128)(2,1)S(1)}, bf16[256,2048]{1,0:T(8,128)(2,1)S(1)}) custom-call(bf16[32,2048]{1,0:T(8,128)(2,1)} %x_ref.1, f32[1,2048]{1,0:T(1,128)} %bitcast.13, s32[2,32]{1,0:T(2,128)} %bitcast.18, f32[2,32]{1,0:T(2,128)} %bitcast.19, f32[1,2048]{1,0:T(1,128)} %bitcast.14, f32[1,2048]{1,0:T(1,128)} %bitcast.15, ...), custom_call_target="tpu_custom_call" | custom-call | tf_op jit(solution)/shard_map/both_modules/pallas_call | solution.py:746
  89.0 1.0 %write_results.1 = (bf16[256,2048]{1,0:T(8,128)(2,1)}, bf16[32,2048]{1,0:T(8,128)(2,1)}) custom-call(bf16[256,2048]{1,0:T(8,128)(2,1)S(1)} %get-tuple-element.4.mixed_ref, bf16[32,2048]{1,0:T(8,128)(2,1)S(1)} %get-tuple-element.5.routed_ref), custom_call_target="tpu_custom_call" | custom-call | tf_op jit(solution)/shard_map/write_results/pallas_call | solution.py:820
